TPU v7x, 32 devices: a whole 2x2x4 slice. The times are simulated.
32 devices in a mesh: tp: 8 (over z, core), dp: 4 (over y, x).
Axes of the slice: x: 2, y: 2, z: 4, core: 2. Of those that a mesh axis runs over, the one named last changes fastest.
Arguments:
- tokens: bfloat16 [128, 2048], P(None, 'dp'), may hold values from -21 to 21
- lengths: int32 [8], P('dp'), may hold values from 1 to 16, 42 in all
- input_norm_scale: float32 [2, 2048], P(None, 'dp'), may hold values from 0.1 to 1.9
- gate_input_weight: bfloat16 [2, 2048, 2, 2048], P(None, 'dp', None, 'tp'), may hold values from -0.125 to 0.125
- maps_weight: bfloat16 [2, 2048, 2, 512], P(None, 'dp', None, 'tp'), may hold values from -0.125 to 0.125
- step_weight: bfloat16 [2, 2048, 32], P(None, 'dp', 'tp'), may hold values from -0.125 to 0.125
- input_tap_weight: bfloat16 [2, 4, 2048], P(None, None, 'tp'), may hold values from -3 to 3
- map_tap_weight: bfloat16 [2, 4, 2, 512], P(None, None, None, 'tp'), may hold values from -3 to 3
- step_size_bias: float32 [2, 32], P(None, 'tp'), may hold values from -4 to -1
- decay_rate_logarithm: float32 [2, 32], P(None, 'tp'), may hold values from -2 to 2.5
- direct_path_weight: float32 [2, 32], P(None, 'tp'), may hold values from 0.25 to 2.5
- head_norm_scale: float32 [2, 2048], P(None, 'tp'), may hold values from 0.1 to 1.9
- output_weight: bfloat16 [2, 2048, 2048], P(None, 'tp', 'dp'), may hold values from -0.125 to 0.125
- convolution_input_cache: bfloat16 [2, 8, 3, 2048], P(None, 'dp', None, 'tp'), may hold values from -6 to 6
- convolution_map_cache: bfloat16 [2, 8, 3, 2, 512], P(None, 'dp', None, None, 'tp'), may hold values from -6 to 6
- recurrent_state: float32 [2, 8, 32, 64, 128], P(None, 'dp', 'tp'), may hold values from -6 to 6
- extra_log_decay: float32 [2, 8, 16, 32], P(None, 'dp', None, 'tp'), may hold values from -0.7 to 0, as said below
Outputs:
- stream_out: float32 [128, 2048], P(None, 'dp')
- conv_input_out: bfloat16 [2, 8, 3, 2048], P(None, 'dp', None, 'tp')
- conv_maps_out: bfloat16 [2, 8, 3, 2, 512], P(None, 'dp', None, None, 'tp')
- ssm_out: float32 [2, 8, 32, 64, 128], P(None, 'dp', 'tp')
Inputs may be any that keep to these rules, and one draw needn't show every extreme that they name: `extra_log_decay`: zero at most slots, a drop of a fifth to a half of the state at a few.
All inputs are finite; a program needn't handle non-finite values. No bound on the sum of `lengths` on one device may be relied on, other than what follows from the above.
Results may differ from a plain program's by a relative error of at most 0.04.
Values may be sent and summed in bfloat16 or wider, within the bound.
A program may use at most 64 MiB of HBM per device.

v0:
```python
import functools

import jax
import jax.numpy as jnp
from jax import lax
from jax.experimental import pallas as pl
from jax.experimental.pallas import tpu as pltpu
from jax.sharding import PartitionSpec as P

EPS = 1e-06
LANES = 128
FRONT = 8
F32, BF16 = jnp.float32, jnp.bfloat16


def up(n):
    return -(-n // LANES) * LANES


def dot(a, b, ca=1, cb=0):
    return lax.dot_general(a, b, (((ca,), (cb,)), ((), ())), preferred_element_type=F32)


def thirds(a):
    high = a.astype(BF16)
    rest = a - high.astype(F32)
    middle = rest.astype(BF16)
    return high, middle, (rest - middle.astype(F32)).astype(BF16)


def grid(n_rows, n_cols):
    return (
        lax.broadcasted_iota(jnp.int32, (n_rows, n_cols), 0),
        lax.broadcasted_iota(jnp.int32, (n_rows, n_cols), 1),
    )


def over(a, n):
    return lax.shift_right_logical(a, jnp.full_like(a, n.bit_length() - 1))


def ones_where(cond):
    return jnp.where(cond, 1.0, 0.0).astype(BF16)


def far_first(k, me, n):
    upper = me // (n // 2)
    mirrored = n - 1 - me
    return upper * (k + (k - me + n) // n) + (1 - upper) * (n - 1 - k - (k - mirrored + n) // n)


def kernel(
    n_tp, n_dp, d_model, heads, groups, slots, seqs, hp_cols, map_cols,
    lens, x, scale, w_pair, w_maps, w_step, tap_u, tap_m, bias, rate, skip, gain, cache_u, cache_m, extra_t,
    state_hbm, wout_hbm,
    stream, kept, ssm,
    a_send, a_recv, m_send, m_recv, h_send, h_recv, o_send, o_recv, n_send, n_recv, padded, step_w, state, wout, taps, par, extra,
    a_ss, a_rs, m_ss, m_rs, h_ss, h_rs, o_ss, o_rs, n_ss, n_rs, s_sem, w_sem,
):
    tp, dp = lax.axis_index("tp"), lax.axis_index("dp")
    layers = w_pair.shape[0]
    rows = seqs * slots
    taps_n = tap_u.shape[1]
    keep = taps_n - 1
    zc = up(hp_cols)
    ng = map_cols // groups
    n_state = state.shape[-1]
    cut = stream.shape[0] // n_tp
    per = rows // cut
    head_size = hp_cols // heads

    state_copy = pltpu.make_async_copy(state_hbm, state, s_sem)
    wout_copy = pltpu.make_async_copy(wout_hbm, wout, w_sem)
    state_copy.start()
    wout_copy.start()
    barrier = pltpu.get_barrier_semaphore()
    for k in range(1, n_dp):
        pl.semaphore_signal(barrier, inc=1, device_id={"dp": lax.rem(dp + k, n_dp)})
    for k in range(1, n_tp):
        pl.semaphore_signal(barrier, inc=1, device_id={"tp": lax.rem(tp + k, n_tp)})

    stream[...] = x[...].astype(F32)
    slot = lax.broadcasted_iota(jnp.int32, (slots, 1), 0)
    mask = jnp.concatenate([(slot < lens[s]).astype(F32) for s in range(seqs)], axis=0)
    lane = lax.broadcasted_iota(jnp.int32, (1, LANES), 1)
    r, c = grid(rows, rows)
    causal = (over(r, slots) == over(c, slots)) & (c <= r)
    tri = ones_where(causal)
    r, c = grid(2 * map_cols, up(2 * map_cols))
    which = over(r, ng) & 1
    sel = ones_where(c == which * map_cols + groups * (r & (ng - 1)) + over(r, 2 * ng))
    r, c = grid(n_tp * 2 * ng, 2 * n_state)
    sel2 = ones_where(c == (over(r, ng) & 1) * n_state + over(r, 2 * ng) * ng + (r & (ng - 1)))
    r, c = grid(LANES, hp_cols)
    ex = ones_where(r == over(c, head_size))
    r, c = grid(hp_cols, LANES)
    ext = ones_where(c == over(r, head_size))
    r, c = grid(hp_cols, hp_cols)
    ones = ones_where(over(r, head_size) == over(c, head_size))
    r, c = grid(LANES, 2 * LANES)
    spread = ones_where(c == 2 * r)
    padded[...] = jnp.zeros_like(padded)
    step_w[...] = jnp.zeros_like(step_w)
    taps[...] = jnp.zeros_like(taps)
    par[...] = jnp.zeros_like(par)
    extra[...] = jnp.zeros_like(extra)
    for l in range(layers):
        step_w[l, :heads, :] = w_step[l]
        taps[l, :taps_n, :hp_cols] = tap_u[l].astype(F32)
        for t in range(taps_n):
            pair = tap_m[l, t].astype(F32)
            for which in range(2):
                at = zc + which * map_cols
                taps[l, t : t + 1, at : at + map_cols] = pair[which : which + 1]
        par[l, 0:1, :heads] = bias[l : l + 1, :]
        par[l, 1:2, :heads] = rate[l : l + 1, :]
        par[l, 2:3, :heads] = skip[l : l + 1, :]
        for s in range(seqs):
            extra[l, :heads, s * slots : (s + 1) * slots] = extra_t[l, s]
    extra_rows = [extra[l].T[:rows] for l in range(layers)]
    skip_x = [sum(dot(piece, ex) for piece in thirds(par[l]))[2:3] for l in range(layers)]
    sends = []

    def copy(src, dst, ss, rs, where):
        return pltpu.make_async_remote_copy(
            src_ref=src, dst_ref=dst, send_sem=ss, recv_sem=rs, device_id=where
        )

    for l in range(layers):
        st = stream[...]
        squares = jnp.sum(st * st, axis=1, keepdims=True)
        normed = (st * scale[l : l + 1, :]).astype(BF16)
        even = jnp.concatenate(
            [dot(normed[:, i : i + LANES], spread) for i in range(0, normed.shape[1], LANES)], axis=1
        )
        odd = pltpu.roll(even, 1, 1)
        pair = dot(jnp.concatenate([even.astype(BF16), odd.astype(BF16)], axis=0), w_pair[l])
        tokens = st.shape[0]
        tail = dot(normed, step_w[l], 1, 1)
        high = squares.astype(BF16).astype(F32)
        tail = jnp.where(lane == LANES - 2, high, jnp.where(lane == LANES - 1, squares - high, tail))
        part = jnp.concatenate(
            [pair[:tokens], pair[tokens:], dot(normed, w_maps[l], 1, 1), tail], axis=1
        ).astype(BF16)
        for b in range(n_dp):
            a_send[l, b] = part[b * rows : (b + 1) * rows]
        if l == 0:
            pl.semaphore_wait(barrier, n_dp - 1 + n_tp - 1)
        flights = []
        for k in range(1, n_dp):
            to = lax.rem(dp + k, n_dp)
            c = copy(a_send.at[l, to], a_recv.at[l, k - 1], a_ss.at[l, k - 1], a_rs.at[l, k - 1], {"dp": to})
            c.start()
            flights.append(c)
        sends += flights
        acc = a_send[l, dp].astype(F32)
        for k, c in enumerate(flights):
            c.wait_recv()
            acc = acc + a_recv[l, k].astype(F32)
        tail = acc[:, acc.shape[1] - LANES :]
        squares = tail[:, LANES - 2 : LANES - 1] + tail[:, LANES - 1 : LANES]
        factor = lax.rsqrt(squares / d_model + EPS)
        proj = (acc * factor).astype(BF16).astype(F32)

        conv_w = taps.shape[2]
        pieces = []
        for s in range(seqs):
            for t in range(keep):
                at = FRONT - keep + t
                padded[s, at : at + 1, :hp_cols] = cache_u[l, t].astype(F32)[s : s + 1]
                pair = cache_m[l, s, t].astype(F32)
                for which in range(2):
                    col = zc + which * map_cols
                    padded[s, at : at + 1, col : col + map_cols] = pair[which : which + 1]
            padded[s, FRONT : FRONT + slots, :] = proj[s * slots : (s + 1) * slots, zc : zc + conv_w]
            total = padded[s, FRONT - keep : FRONT - keep + slots, :] * taps[l, 0:1, :]
            for t in range(1, taps_n):
                at = FRONT - keep + t
                total = total + padded[s, at : at + slots, :] * taps[l, t : t + 1, :]
            pieces.append(total)
        filtered = jnp.concatenate(pieces, axis=0)
        filtered = filtered * jax.nn.sigmoid(filtered)
        maps = filtered[:, conv_w - up(2 * map_cols) :].astype(BF16)
        sorted_maps = dot(sel, maps, 1, 1)
        for g in range(groups):
            m_send[l, g] = sorted_maps[g * 2 * ng : (g + 1) * 2 * ng, :].astype(BF16)

        def group_of(rank):
            return rank * heads // (heads * n_tp // groups)

        flights = []
        for k in range(n_tp - 1):
            to = far_first(k, tp, n_tp)
            c = copy(m_send.at[l, group_of(to)], m_recv.at[l, tp], m_ss.at[l, k], m_rs.at[l, tp], {"tp": to})
            c.start()
            sends.append(c)
        m_recv[l, tp] = m_send[l, group_of(tp)]

        for s in range(seqs):
            pick = lax.broadcasted_iota(jnp.int32, (8, FRONT + slots), 0)
            place = lax.broadcasted_iota(jnp.int32, (8, FRONT + slots), 1)
            chooser = ((place == pick + lens[s] + (FRONT - keep)) & (pick < keep)).astype(BF16)
            kept[l, s] = dot(chooser, padded[s].astype(BF16)).astype(BF16)
        raw = proj[:, proj.shape[1] - LANES :] + par[l, 0:1, :]
        step = (jnp.maximum(raw, 0.0) + jnp.log1p(jnp.exp(-jnp.abs(raw)))) * mask
        step = jnp.where(lane < heads, step, 0.0)
        logdec = extra_rows[l] * mask - step * jnp.exp(par[l, 1:2, :])
        logdec = jnp.where(lane < heads, logdec, 0.0)
        parts = dot(tri, jnp.concatenate(thirds(logdec), axis=1))
        sums = parts[:, :LANES] + parts[:, LANES : 2 * LANES] + parts[:, 2 * LANES :]
        sums_t = sums.T
        step_t = step.T
        sums_parts, step_parts = thirds(sums), thirds(step)
        both = dot(jnp.concatenate(sums_parts + step_parts, axis=0), ex)
        sums_x = both[:rows] + both[rows : 2 * rows] + both[2 * rows : 3 * rows]
        step_x = both[3 * rows : 4 * rows] + both[4 * rows : 5 * rows] + both[5 * rows :]
        inp = filtered[:, :hp_cols]
        gate = proj[:, :hp_cols]
        last_x = jnp.concatenate(
            [
                jnp.broadcast_to(sums_x[(s + 1) * slots - 1 : (s + 1) * slots, :], (slots, hp_cols))
                for s in range(seqs)
            ],
            axis=0,
        )
        weighted = (jnp.exp(last_x - sums_x) * step_x * inp).astype(BF16)
        inp_b = inp.astype(BF16)
        grow = jnp.exp(sums_x)
        direct = skip_x[l] * inp
        gate = gate * jax.nn.sigmoid(gate)
        rows_sum = sum(dot(ext, piece, 1, 1) for piece in sums_parts)
        segs = []
        for h in range(heads):
            gap = sums[:, h : h + 1] - sums_t[h : h + 1, :]
            segs.append(jnp.exp(jnp.where(causal, gap, -jnp.inf)) * step_t[h : h + 1, :])

        if l == 0:
            state_copy.wait()
            wout_copy.wait()
        for k in range(1, n_tp):
            src = lax.rem(tp + n_tp - k, n_tp)
            copy(m_send.at[l, 0], m_recv.at[l, src], m_ss.at[l, 0], m_rs.at[l, src], {"tp": src}).wait_recv()
        got = m_recv[l].astype(F32).reshape(n_tp * 2 * ng, rows)
        both_maps = dot(got.T.astype(BF16), sel2).astype(BF16)
        b_map, c_map = both_maps[:, :n_state], both_maps[:, n_state:]
        cross = dot(c_map, b_map, 1, 1)
        within = jnp.concatenate(
            [
                dot((cross * segs[h]).astype(BF16), inp_b[:, h * head_size : (h + 1) * head_size])
                for h in range(heads)
            ],
            axis=1,
        )
        carried = jnp.concatenate(
            [
                dot(c_map[s * slots : (s + 1) * slots], state[l, s].astype(BF16), 1, 1)
                for s in range(seqs)
            ],
            axis=0,
        )
        read = (within + carried * grow + direct) * gate
        power = read * read
        p_hi = power.astype(BF16)
        p_lo = (power - p_hi.astype(F32)).astype(BF16)
        mean = (dot(p_hi, ones) + dot(p_lo, ones)) / head_size
        headout = (read * lax.rsqrt(mean + EPS) * gain[l : l + 1, :] * mask).astype(BF16)
        h_send[l] = headout
        flights = []
        for k in range(1, n_dp):
            to = lax.rem(dp + k, n_dp)
            c = copy(h_send.at[l], h_recv.at[l, k - 1], h_ss.at[l, k - 1], h_rs.at[l, k - 1], {"dp": to})
            c.start()
            flights.append(c)
        sends += flights

        def push(value, block):
            out = dot(value, wout[l]).astype(BF16)
            for i in range(per):
                to = block * per + i
                o_send[l, to] = out[i * cut : (i + 1) * cut]

                @pl.when(to != tp)
                def _():
                    copy(o_send.at[l, to], o_recv.at[l, tp], o_ss.at[l, to], o_rs.at[l, tp], {"tp": to}).start()

        push(headout, dp)
        for s in range(seqs):
            at = slice(s * slots, (s + 1) * slots)
            fresh = dot(weighted[at], b_map[at], 0, 0)
            end = (s + 1) * slots - 1
            ssm[l, s] = jnp.exp(rows_sum[:, end : end + 1]) * state[l, s] + fresh
        for k, c in enumerate(flights):
            c.wait_recv()
            push(h_recv[l, k], lax.rem(dp + n_dp - k - 1, n_dp))
        total = o_send[l, tp].astype(F32)
        for k in range(1, n_tp):
            src = lax.rem(tp + n_tp - k, n_tp)
            copy(o_send.at[l, src], o_recv.at[l, src], o_ss.at[l, src], o_rs.at[l, src], {"tp": src}).wait_recv()
            total = total + o_recv[l, src].astype(F32)
        fresh = total.astype(BF16)
        n_send[l] = fresh
        n_recv[l, tp] = fresh
        for k in range(n_tp - 1):
            to = far_first(k, tp, n_tp)
            c = copy(n_send.at[l], n_recv.at[l, tp], n_ss.at[l, k], n_rs.at[l, tp], {"tp": to})
            c.start()
            sends.append(c)
        for k in range(1, n_tp):
            src = lax.rem(tp + n_tp - k, n_tp)
            copy(n_send.at[l], n_recv.at[l, src], n_ss.at[l, 0], n_rs.at[l, src], {"tp": src}).wait_recv()
        stream[...] += n_recv[l].astype(F32).reshape(stream.shape)

    for c in sends:
        c.wait_send()
    for l in range(layers):
        for k in range(1, n_tp):
            to = lax.rem(tp + k, n_tp)
            copy(o_send.at[l, to], o_recv.at[l, tp], o_ss.at[l, to], o_rs.at[l, tp], {"tp": to}).wait_send()


def body(
    n_tp, n_dp,
    tokens, lengths, input_norm_scale, gate_input_weight, maps_weight, step_weight,
    input_tap_weight, map_tap_weight, step_size_bias, decay_rate_logarithm, direct_path_weight,
    head_norm_scale, output_weight, convolution_input_cache, convolution_map_cache,
    recurrent_state, extra_log_decay,
):
    layers, seqs, slots, heads = extra_log_decay.shape
    head_size, n_state = recurrent_state.shape[3:]
    hp_cols = heads * head_size
    map_cols = maps_weight.shape[3]
    groups = map_cols * n_tp // n_state
    ng = map_cols // groups
    rows = seqs * slots
    d_here = tokens.shape[1]
    keep = convolution_input_cache.shape[2]

    def wide(a):
        pad = up(a.shape[-1]) - a.shape[-1]
        return a if pad == 0 else jnp.pad(a, [(0, 0)] * (a.ndim - 1) + [(0, pad)])

    w_pair = wide(gate_input_weight.reshape(layers, 2 * d_here, hp_cols))
    w_maps = jnp.transpose(maps_weight, (0, 2, 3, 1)).reshape(layers, 2 * map_cols, d_here)
    if up(2 * map_cols) > 2 * map_cols:
        w_maps = jnp.pad(w_maps, ((0, 0), (0, up(2 * map_cols) - 2 * map_cols), (0, 0)))
    w_step = jnp.transpose(step_weight, (0, 2, 1))
    cache_u = jnp.transpose(convolution_input_cache, (0, 2, 1, 3))
    extra_t = jnp.transpose(extra_log_decay, (0, 1, 3, 2))
    state = recurrent_state.reshape(layers, seqs, hp_cols, n_state)

    vmem = pl.BlockSpec(memory_space=pltpu.VMEM)
    wide_cols = 2 * up(hp_cols) + up(2 * map_cols) + LANES
    anywhere = pl.BlockSpec(memory_space=pl.ANY)
    conv_w = up(hp_cols) + up(2 * map_cols)
    cut = tokens.shape[0] // n_tp
    sems = lambda n: pltpu.SemaphoreType.DMA((layers, n))
    args = [tokens, input_norm_scale, w_pair, w_maps, w_step, input_tap_weight,
        map_tap_weight, step_size_bias, decay_rate_logarithm, direct_path_weight, head_norm_scale,
        cache_u, convolution_map_cache, extra_t]
    stream, kept, ssm = pl.pallas_call(
        functools.partial(
            kernel, n_tp, n_dp, d_here * n_dp, heads, groups, slots, seqs, hp_cols, map_cols
        ),
        out_shape=(
            jax.ShapeDtypeStruct(tokens.shape, F32),
            jax.ShapeDtypeStruct((layers, seqs, 8, conv_w), BF16),
            jax.ShapeDtypeStruct(state.shape, F32),
        ),
        in_specs=[pl.BlockSpec(memory_space=pltpu.SMEM)] + [vmem] * len(args) + [anywhere] * 2,
        out_specs=(vmem, vmem, vmem),
        scratch_shapes=[
            pltpu.VMEM((layers, n_dp, rows, wide_cols), BF16),
            pltpu.VMEM((layers, n_dp - 1, rows, wide_cols), BF16),
            pltpu.VMEM((layers, groups, 2 * ng, rows), BF16),
            pltpu.VMEM((layers, n_tp, 2 * ng, rows), BF16),
            pltpu.VMEM((layers, rows, hp_cols), BF16),
            pltpu.VMEM((layers, n_dp - 1, rows, hp_cols), BF16),
            pltpu.VMEM((layers, n_tp, cut, d_here), BF16),
            pltpu.VMEM((layers, n_tp, cut, d_here), BF16),
            pltpu.VMEM((layers, cut, d_here), BF16),
            pltpu.VMEM((layers, n_tp, cut, d_here), BF16),
            pltpu.VMEM((seqs, FRONT + slots, conv_w), F32),
            pltpu.VMEM((layers, LANES, d_here), BF16),
            pltpu.VMEM(state.shape, F32),
            pltpu.VMEM(output_weight.shape, BF16),
            pltpu.VMEM((layers, 8, conv_w), F32),
            pltpu.VMEM((layers, 8, LANES), F32),
            pltpu.VMEM((layers, LANES, LANES), F32),
            sems(n_dp - 1), sems(n_dp - 1), sems(n_tp - 1), sems(n_tp), sems(n_dp - 1),
            sems(n_dp - 1), sems(n_tp), sems(n_tp), sems(n_tp - 1), sems(n_tp),
            pltpu.SemaphoreType.DMA, pltpu.SemaphoreType.DMA,
        ],
        compiler_params=pltpu.CompilerParams(
            collective_id=0, has_side_effects=True, vmem_limit_bytes=48 * 2**20
        ),
        name="mixer",
    )(lengths, *args, state, output_weight)
    conv_in = kept[:, :, :keep, :hp_cols]
    start = conv_w - up(2 * map_cols)
    conv_maps = kept[:, :, :keep, start : start + 2 * map_cols].reshape(
        layers, seqs, keep, 2, map_cols
    )
    return stream, conv_in, conv_maps, ssm.reshape(recurrent_state.shape)


def solution(mesh):
    placed = (
        P(None, "dp"),
        P("dp"),
        P(None, "dp"),
        P(None, "dp", None, "tp"),
        P(None, "dp", None, "tp"),
        P(None, "dp", "tp"),
        P(None, None, "tp"),
        P(None, None, None, "tp"),
        P(None, "tp"),
        P(None, "tp"),
        P(None, "tp"),
        P(None, "tp"),
        P(None, "tp", "dp"),
        P(None, "dp", None, "tp"),
        P(None, "dp", None, None, "tp"),
        P(None, "dp", "tp", None, None),
        P(None, "dp", None, "tp"),
    )
    return jax.shard_map(
        functools.partial(body, mesh.shape["tp"], mesh.shape["dp"]),
        mesh=mesh,
        in_specs=placed,
        out_specs=(
            P(None, "dp"),
            P(None, "dp", None, "tp"),
            P(None, "dp", None, None, "tp"),
            P(None, "dp", "tp", None, None),
        ),
        check_vma=False,
    )
```

profile of v0, /device:TPU:0, one launch (start us, length us, event | category | flops | bytes accessed | tf_op | source)
XLA Modules:
  0.0 54.4 jit_solution(1157446357131992755)
XLA Ops:
  0.6 0.0 copy-start
  0.6 0.0 copy-start.1
  0.7 0.0 copy-start.2
  0.7 0.0 copy-start.3
  0.7 0.0 copy-start.4
  0.7 0.0 copy-start.5
  0.7 0.0 copy-start.6
  0.7 0.0 copy-start.7
  0.7 0.0 copy-start.8
  0.7 0.0 copy-start.9
  0.7 0.0 copy-start.10
  0.7 0.0 copy-start.11
  0.8 0.0 copy-start.12
  0.8 0.0 copy-start.13
  0.8 0.0 copy-start.14
  0.8 0.0 copy-start.15
  0.8 1.5 %reshape.23.w_pair = bf16[2,1024,256]{2,1,0:T(8,128)(2,1)S(1)} reshape(bf16[2,512,2,256]{3,2,1,0:T(2,128)(2,1)} %param.20) | data formatting | bytes 2097152 | tf_op jit(solution)/shard_map/reshape | solution.py:342
  2.4 0.0 copy-done
  2.4 0.0 copy-done.1
  2.4 0.0 copy-done.2
  2.4 0.0 copy-done.3
  2.4 0.0 copy-done.4
  2.4 0.0 copy-done.5
  2.4 0.0 copy-done.6
  2.4 0.0 copy-done.7
  2.4 0.0 copy-done.8
  2.4 0.0 copy-done.9
  2.5 0.0 copy-done.10
  2.5 0.0 copy-done.11
  2.5 0.0 copy-done.12
  2.5 0.0 copy-done.13
  2.5 0.0 copy-done.14
  2.5 0.0 copy-done.15
  2.5 49.1 %mixer.1 = (f32[128,512]{1,0:T(8,128)S(1)}, bf16[2,2,8,384]{3,2,1,0:T(8,128)(2,1)S(1)}, f32[2,2,256,128]{3,2,1,0:T(8,128)S(1)}) custom-call(s32[2]{0:T(128)S(1)} %copy-done.15, bf16[128,512]{1,0:T(8,128)(2,1)S(1)} %copy-done.3, f32[2,512]{1,0:T(2,128)S(1)} %copy-done.8, bf16[2,1024,256]{2,1,0:T(8,128)(2,1)S(1)} %reshape.23.w_pair, ...), custom_call_target="tpu_custom_call" | custom-call | tf_op jit(solution)/shard_map/mixer/pallas_call | solution.py:360
  51.6 0.6 %copy.23 = bf16[2,2,3,256]{3,1,2,0:T(2,128)(2,1)} copy(bf16[2,2,3,256]{3,2,1,0:T(4,128)(2,1)S(1)} %slice.6) | data formatting | bytes 12288
  52.2 0.7 %reshape.28 = bf16[2,2,3,2,64]{4,3,2,1,0:T(2,128)(2,1)} reshape(bf16[2,2,3,128]{3,2,1,0:T(4,128)(2,1)S(1)} %slice.7) | data formatting | bytes 6144 | tf_op jit(solution)/shard_map/reshape | solution.py:400
  52.9 0.7 %copy.28 = f32[128,512]{1,0:T(8,128)} copy(f32[128,512]{1,0:T(8,128)S(1)} %get-tuple-element.22) | data formatting | bytes 524288
  53.6 0.8 %copy.29 = f32[2,2,4,64,128]{4,3,2,1,0:T(8,128)} copy(f32[2,2,4,64,128]{4,3,2,1,0:T(8,128)S(1)} %bitcast.9) | data formatting | bytes 1048576
  (2 shorter events, 0.0 us)
Async XLA Ops:
  0.6 1.7 %copy-start = (f32[2,2,4,64,128]{4,3,2,1,0:T(8,128)S(1)}, f32[2,2,4,64,128]{4,3,2,1,0:T(8,128)}, u32[]{:S(2)}) copy-start(f32[2,2,4,64,128]{4,3,2,1,0:T(8,128)} %param.32) | copy-start | bytes 1572868
  0.6 1.7 %copy-start.1 = (bf16[2,256,512]{2,1,0:T(8,128)(2,1)S(1)}, bf16[2,256,512]{2,1,0:T(8,128)(2,1)}, u32[]{:S(2)}) copy-start(bf16[2,256,512]{2,1,0:T(8,128)(2,1)} %wout_hbm.1) | copy-start | bytes 1572868
  0.7 1.7 %copy-start.2 = (bf16[2,512,2,64]{1,3,2,0:T(8,128)(2,1)S(1)}, bf16[2,512,2,64]{1,3,2,0:T(8,128)(2,1)}, u32[]{:S(2)}) copy-start(bf16[2,512,2,64]{1,3,2,0:T(8,128)(2,1)} %param.21) | copy-start | bytes 786436
  0.7 1.7 %copy-start.3 = (bf16[128,512]{1,0:T(8,128)(2,1)S(1)}, bf16[128,512]{1,0:T(8,128)(2,1)}, u32[]{:S(2)}) copy-start(bf16[128,512]{1,0:T(8,128)(2,1)} %x.1) | copy-start | bytes 393220
  0.7 1.7 %copy-start.4 = (bf16[2,512,4]{1,2,0:T(4,128)(2,1)S(1)}, bf16[2,512,4]{1,2,0:T(4,128)(2,1)}, u32[]{:S(2)}) copy-start(bf16[2,512,4]{1,2,0:T(4,128)(2,1)} %param.22) | copy-start | bytes 24580
  0.7 1.7 %copy-start.5 = (f32[2,2,16,4]{2,3,1,0:T(4,128)S(1)}, f32[2,2,16,4]{2,3,1,0:T(4,128)}, u32[]{:S(2)}) copy-start(f32[2,2,16,4]{2,3,1,0:T(4,128)} %param.33) | copy-start | bytes 3076
  0.7 1.7 %copy-start.6 = (bf16[2,2,3,256]{3,1,2,0:T(2,128)(2,1)S(1)}, bf16[2,2,3,256]{3,1,2,0:T(2,128)(2,1)}, u32[]{:S(2)}) copy-start(bf16[2,2,3,256]{3,1,2,0:T(2,128)(2,1)} %param.30) | copy-start | bytes 18436
  0.7 1.7 %copy-start.7 = (bf16[2,2,3,2,64]{4,3,2,1,0:T(2,128)(2,1)S(1)}, bf16[2,2,3,2,64]{4,3,2,1,0:T(2,128)(2,1)}, u32[]{:S(2)}) copy-start(bf16[2,2,3,2,64]{4,3,2,1,0:T(2,128)(2,1)} %cache_m.1) | copy-start | bytes 9220
  0.7 1.7 %copy-start.8 = (f32[2,512]{1,0:T(2,128)S(1)}, f32[2,512]{1,0:T(2,128)}, u32[]{:S(2)}) copy-start(f32[2,512]{1,0:T(2,128)} %scale.1) | copy-start | bytes 12292
  0.7 1.7 %copy-start.9 = (bf16[2,4,256]{2,1,0:T(4,128)(2,1)S(1)}, bf16[2,4,256]{2,1,0:T(4,128)(2,1)}, u32[]{:S(2)}) copy-start(bf16[2,4,256]{2,1,0:T(4,128)(2,1)} %tap_u.1) | copy-start | bytes 12292
  0.7 1.7 %copy-start.10 = (bf16[2,4,2,64]{3,2,1,0:T(2,128)(2,1)S(1)}, bf16[2,4,2,64]{3,2,1,0:T(2,128)(2,1)}, u32[]{:S(2)}) copy-start(bf16[2,4,2,64]{3,2,1,0:T(2,128)(2,1)} %tap_m.1) | copy-start | bytes 6148
  0.7 1.7 %copy-start.11 = (f32[2,256]{1,0:T(2,128)S(1)}, f32[2,256]{1,0:T(2,128)}, u32[]{:S(2)}) copy-start(f32[2,256]{1,0:T(2,128)} %gain.1) | copy-start | bytes 6148
  0.8 1.7 %copy-start.12 = (f32[2,4]{1,0:T(2,128)S(1)}, f32[2,4]{1,0:T(2,128)}, u32[]{:S(2)}) copy-start(f32[2,4]{1,0:T(2,128)} %bias.1) | copy-start | bytes 100
  0.8 1.7 %copy-start.13 = (f32[2,4]{1,0:T(2,128)S(1)}, f32[2,4]{1,0:T(2,128)}, u32[]{:S(2)}) copy-start(f32[2,4]{1,0:T(2,128)} %rate.1) | copy-start | bytes 100
  0.8 1.7 %copy-start.14 = (f32[2,4]{1,0:T(2,128)S(1)}, f32[2,4]{1,0:T(2,128)}, u32[]{:S(2)}) copy-start(f32[2,4]{1,0:T(2,128)} %skip.1) | copy-start | bytes 100
  0.8 1.7 %copy-start.15 = (s32[2]{0:T(128)S(1)}, s32[2]{0:T(128)}, u32[]{:S(2)}) copy-start(s32[2]{0:T(128)} %lens.1) | copy-start | bytes 28
where the time goes:
time: 54.5 us; the launch traced here: 54.4 us
  Pallas kernels  49.1 us (90%)
  local copies, waits for them, and re-layouts  4.4 us (8%)
  between operations  0.92 us (2%)
    pallas_call x1, Pallas kernels, body(): pl.pallas_call(functools.partial(kernel, n_tp, n_dp, d_here * n_dp, heads...  49.1 us
    unnamed x35, local copies, waits for them, and re-layouts  2.16 us
    reshape x1, local copies, waits for them, and re-layouts, body(): w_pair = wide(gate_input_weight.reshape(layers, 2 * d_here, hp_cols))  1.55 us

commit v1 on v0

--- a/solution.py
+++ b/solution.py
@@ -49,7 +49,7 @@
     return upper * (k + (k - me + n) // n) + (1 - upper) * (n - 1 - k - (k - mirrored + n) // n)
 
 
-def kernel(
+def general_kernel(
     n_tp, n_dp, d_model, heads, groups, slots, seqs, hp_cols, map_cols,
     lens, x, scale, w_pair, w_maps, w_step, tap_u, tap_m, bias, rate, skip, gain, cache_u, cache_m, extra_t,
     state_hbm, wout_hbm,
@@ -318,7 +318,7 @@
             copy(o_send.at[l, to], o_recv.at[l, tp], o_ss.at[l, to], o_rs.at[l, tp], {"tp": to}).wait_send()
 
 
-def body(
+def general_body(
     n_tp, n_dp,
     tokens, lengths, input_norm_scale, gate_input_weight, maps_weight, step_weight,
     input_tap_weight, map_tap_weight, step_size_bias, decay_rate_logarithm, direct_path_weight,
@@ -359,7 +359,7 @@
         cache_u, convolution_map_cache, extra_t]
     stream, kept, ssm = pl.pallas_call(
         functools.partial(
-            kernel, n_tp, n_dp, d_here * n_dp, heads, groups, slots, seqs, hp_cols, map_cols
+            general_kernel, n_tp, n_dp, d_here * n_dp, heads, groups, slots, seqs, hp_cols, map_cols
         ),
         out_shape=(
             jax.ShapeDtypeStruct(tokens.shape, F32),
@@ -403,6 +403,589 @@
     return stream, conv_in, conv_maps, ssm.reshape(recurrent_state.shape)
 
 
+def peers(n, order):
+    return [k for k in order if 0 < k < n] + [k for k in range(1, n) if k not in order]
+
+
+def kernel(
+    n_tp, n_dp, d_model, groups, shapes,
+    *refs,
+):
+    names = (
+        "lens", "x", "scale", "gate", "w_maps", "w_step", "tap_u", "tap_m", "bias", "rate", "skip", "gain",
+        "cache_u", "cache_m", "extra_t", "state", "wout",
+    )
+    hbm = dict(zip(names, refs[: len(names)]))
+    (
+        stream, kept_u, kept_m, ssm,
+        lens, x, scale, w_gate, w_maps, w_step, tap_u, tap_m, bias, rate, skip, gain, cache_u, cache_m, extra_t, state,
+        wout, in_sem, g_sem,
+        a_send, a_recv, m_send, m_recv, c_send, c_recv, h_recv, o_send, o_recv, nb,
+        padded, padded_m, mrow, mrows, step_w, w_sorted, taps, par, extra,
+        a_ss, a_rs, m_ss, m_rs, c_ss, c_rs, h_ss, h_rs, o_ss, o_rs, n_ss, n_rs, w_ss, w_rs,
+    ) = refs[len(names) :]
+    layers, seqs, slots, heads, head_size, n_state, hp_cols, map_cols = shapes
+    tp, dp = lax.axis_index("tp"), lax.axis_index("dp")
+    rows = seqs * slots
+    taps_n = tap_u.shape[1]
+    keep = taps_n - 1
+    ng = map_cols // groups
+    pair_cols = 2 * ng
+    quads = LANES // pair_cols
+    d_here = x.shape[1]
+    half = d_here // 2
+    tokens = x.shape[0]
+    side = lax.rem(tp, 2)
+    zed = lax.div(tp, 2)
+    n_z = n_tp // 2
+    every = n_tp * n_dp
+    me = dp * n_tp + tp
+    dp_peers = peers(n_dp, (3, 1, 2))
+    near_first = peers(n_dp, (1, 2, 3))
+    z_peers = peers(n_z, (3, 2, 1))
+
+    def remote(src, dst, ss, rs, where):
+        return pltpu.make_async_remote_copy(
+            src_ref=src, dst_ref=dst, send_sem=ss, recv_sem=rs, device_id=where
+        )
+
+    barrier = pltpu.get_barrier_semaphore()
+    others = [
+        (i, j) for i in [*peers(n_tp, (6, 7, 4, 5, 2, 3, 1)), 0] for j in [*dp_peers, 0] if i or j
+    ]
+
+    def at(i, j):
+        return {"tp": jnp.bitwise_xor(tp, i), "dp": jnp.bitwise_xor(dp, j)}
+
+    for i, j in others:
+        pl.semaphore_signal(barrier, inc=1, device_id=at(i, j))
+
+    local = {}
+    pairs = dict(
+        x=x, scale=scale, w_maps=w_maps, w_step=w_step, lens=lens, tap_u=tap_u, tap_m=tap_m, bias=bias, rate=rate,
+        skip=skip, gain=gain, cache_u=cache_u, cache_m=cache_m, extra_t=extra_t, state=state,
+    )
+    for n, name in enumerate(pairs):
+        local[name] = pltpu.make_async_copy(hbm[name], pairs[name], in_sem.at[n])
+    mine = pl.ds(pl.multiple_of(side * half, LANES), half)
+    theirs = pl.ds(pl.multiple_of((1 - side) * half, LANES), half)
+    local["wout"] = pltpu.make_async_copy(hbm["wout"].at[:, :, mine], wout.at[:, 0], in_sem.at[len(pairs)])
+    gate_copies = [
+        [
+            pltpu.make_async_copy(
+                hbm["gate"].at[l, :, :, i : i + LANES], w_gate.at[l, i // LANES], g_sem.at[l, i // LANES]
+            )
+            for i in range(0, hp_cols, LANES)
+        ]
+        for l in range(layers)
+    ]
+    first = ("x", "scale", "w_maps", "w_step")
+    for name in first:
+        local[name].start()
+    for c in gate_copies[0]:
+        c.start()
+    for name in local:
+        if name not in first:
+            local[name].start()
+    for l in range(1, layers):
+        for c in gate_copies[l]:
+            c.start()
+
+    lane = lax.broadcasted_iota(jnp.int32, (1, LANES), 1)
+    r, c = grid(LANES, 4 * LANES)
+    spread = ones_where(c == jnp.where(c < 2 * LANES, 2 * r, 2 * LANES + 2 * r + 1))
+    r, c = grid(LANES, LANES)
+    place = (c + LANES - ng * tp) & (LANES - 1)
+    wanted = (over(place, ng) & 1) * map_cols + groups * (place & (ng - 1)) + over(place, pair_cols)
+    sorter = ones_where(r == wanted)
+    home = over((lane + LANES - ng * tp) & (LANES - 1), pair_cols)
+    step_w[...] = jnp.zeros_like(step_w)
+    gate_rows = w_gate.reshape(layers, hp_cols // LANES, 2 * d_here, LANES)
+
+    def group_of(rank):
+        return rank * groups // n_tp
+
+    def project(l):
+        st = stream[...]
+        squares = jnp.sum(st * st, axis=1, keepdims=True)
+        normed = (st * scale[l : l + 1, :]).astype(BF16)
+        raw = dot(normed, w_sorted[l], 1, 1)
+        turned = [raw if k == 0 else pltpu.roll(raw, k * pair_cols, 1) for k in range(quads)]
+        turned = [t.reshape(n_dp, quads, 8, LANES) for t in turned]
+        for g in range(groups):
+            piece = turned[(0 - g) % quads][:, 0]
+            for q in range(1, quads):
+                piece = jnp.where((home == q)[None], turned[(q - g) % quads][:, q], piece)
+            m_send[l, g] = piece.astype(BF16)
+        return normed, squares, raw
+
+    def send_maps(l):
+        for i, j in others:
+            to = at(i, j)
+            remote(
+                m_send.at[l, group_of(to["tp"]), to["dp"]], m_recv.at[l, me], m_ss.at[l], m_rs.at[l], to
+            ).start()
+        m_recv[l, me] = m_send[l, group_of(tp), dp]
+
+    def project_rest(l, normed, squares, raw):
+        spreads = [dot(normed[:, i : i + LANES], spread).astype(BF16) for i in range(0, d_here, LANES)]
+        even = jnp.concatenate([s[:, : 2 * LANES] for s in spreads], axis=1)
+        odd = jnp.concatenate([s[:, 2 * LANES :] for s in spreads], axis=1)
+        for c in gate_copies[l]:
+            c.wait()
+        weight = jnp.concatenate([gate_rows[l, i] for i in range(hp_cols // LANES)], axis=1)
+        both = dot(jnp.concatenate([odd, even], axis=0), weight)
+        tail = dot(normed, step_w[l], 1, 1)
+        high = squares.astype(BF16).astype(F32)
+        tail = jnp.where(lane == LANES - 2, high, jnp.where(lane == LANES - 1, squares - high, tail))
+        one = jnp.concatenate([both[:tokens], tail], axis=1).astype(BF16)
+        two = jnp.concatenate([both[tokens:], raw], axis=1).astype(BF16)
+        for b in range(n_dp):
+            a_send[l, 0, b] = one[b * rows : (b + 1) * rows]
+            a_send[l, 1, b] = two[b * rows : (b + 1) * rows]
+
+    def send_rest(l):
+        for p in range(2):
+            for k in dp_peers:
+                to = jnp.bitwise_xor(dp, k)
+                remote(
+                    a_send.at[l, p, to], a_recv.at[l, p, k - 1], a_ss.at[l, p, k - 1], a_rs.at[l, p, k - 1], {"dp": to}
+                ).start()
+
+    def await_rest(l, p):
+        acc = a_send[l, p, dp].astype(F32)
+        for k in dp_peers:
+            remote(
+                a_send.at[l, p, 0], a_recv.at[l, p, k - 1], a_ss.at[l, p, k - 1], a_rs.at[l, p, k - 1],
+                {"dp": jnp.bitwise_xor(dp, k)},
+            ).wait_recv()
+        for k in range(1, n_dp):
+            acc = acc + a_recv[l, p, k - 1].astype(F32)
+        return acc
+
+    sends = []
+    for name in first:
+        local[name].wait()
+    for l in range(layers):
+        step_w[l, :heads, :] = w_step[l]
+    w_sorted[0] = dot(sorter, w_maps[0], 0, 0).astype(BF16)
+    stream[...] = x[...].astype(F32)
+
+    for l in range(layers):
+        normed, squares, raw = project(l)
+        if l == 0:
+            project_rest(l, normed, squares, raw)
+            pl.semaphore_wait(barrier, every - 1)
+        send_maps(l)
+        if l > 0:
+            project_rest(l, normed, squares, raw)
+        send_rest(l)
+
+        if l == 0:
+            for n in range(len(pairs) + 1):
+                name = [*pairs, "wout"][n]
+                if name not in first:
+                    local[name].wait()
+            swap = remote(hbm["wout"].at[:, :, theirs], wout.at[:, 1], w_ss, w_rs, {"tp": jnp.bitwise_xor(tp, 1)})
+            swap.start()
+            for i in range(1, layers):
+                w_sorted[i] = dot(sorter, w_maps[i], 0, 0).astype(BF16)
+            per_layer = seqs * keep + taps_n
+            mrow[...] = jnp.zeros_like(mrow)
+            for i in range(layers):
+                for s in range(seqs):
+                    for t in range(keep):
+                        pair = cache_m[i, s, t].astype(F32)
+                        n = i * per_layer + s * keep + t
+                        for which in range(2):
+                            mrow[which, n : n + 1, :map_cols] = pair[which : which + 1]
+                for t in range(taps_n):
+                    pair = tap_m[i, t].astype(F32)
+                    n = i * per_layer + seqs * keep + t
+                    for which in range(2):
+                        mrow[which, n : n + 1, :map_cols] = pair[which : which + 1]
+            n_rows = mrow.shape[1]
+            r, c = grid(LANES, groups * LANES)
+            n = (c & (LANES - 1)) - ng * tp
+            chosen = (n >= 0) & (n < ng) & (r == groups * n + over(c, LANES))
+            packed = dot(mrow[...].reshape(2 * n_rows, LANES).astype(BF16), ones_where(chosen)).astype(BF16)
+            for g in range(groups):
+                c_send[g] = packed[:, g * LANES : (g + 1) * LANES]
+            for k in peers(n_tp, (6, 7, 4, 5, 2, 3, 1)):
+                to = jnp.bitwise_xor(tp, k)
+                c = remote(c_send.at[group_of(to)], c_recv.at[k], c_ss.at[k - 1], c_rs.at[k - 1], {"tp": to})
+                c.start()
+                sends.append(c)
+            c_recv[0] = c_send[group_of(tp)]
+
+            slot = lax.broadcasted_iota(jnp.int32, (slots, 1), 0)
+            mask = jnp.concatenate([(slot < lens[s]).astype(F32) for s in range(seqs)], axis=0)
+            r, c = grid(rows, rows)
+            causal = (over(r, slots) == over(c, slots)) & (c <= r)
+            tri = ones_where(causal)
+            r, c = grid(LANES, hp_cols)
+            ex = ones_where(r == over(c, head_size))
+            r, c = grid(hp_cols, LANES)
+            ext = ones_where(c == over(r, head_size))
+            r, c = grid(hp_cols, hp_cols)
+            ones = ones_where(over(r, head_size) == over(c, head_size))
+            padded[...] = jnp.zeros_like(padded)
+            padded_m[...] = jnp.zeros_like(padded_m)
+            taps[...] = jnp.zeros_like(taps)
+            par[...] = jnp.zeros_like(par)
+            extra[...] = jnp.zeros_like(extra)
+            for i in range(layers):
+                taps[i, :taps_n, :] = tap_u[i].astype(F32)
+                par[i, 0:1, :heads] = bias[i : i + 1, :]
+                par[i, 1:2, :heads] = rate[i : i + 1, :]
+                par[i, 2:3, :heads] = skip[i : i + 1, :]
+                for s in range(seqs):
+                    extra[i, :heads, s * slots : (s + 1) * slots] = extra_t[i, s]
+                    for t in range(keep):
+                        n = FRONT - keep + t
+                        padded[i, s, n : n + 1, :] = cache_u[i, t].astype(F32)[s : s + 1]
+            extra_rows = [extra[i].T[:rows] for i in range(layers)]
+            skip_x = [sum(dot(piece, ex) for piece in thirds(par[i]))[2:3] for i in range(layers)]
+
+        def convolve(pad, weights):
+            pieces = []
+            for s in range(seqs):
+                total = pad[l, s, FRONT - keep : FRONT - keep + slots, :] * weights[0:1]
+                for t in range(1, taps_n):
+                    n = FRONT - keep + t
+                    total = total + pad[l, s, n : n + slots, :] * weights[t : t + 1]
+                pieces.append(total)
+            out = jnp.concatenate(pieces, axis=0)
+            return out * jax.nn.sigmoid(out)
+
+        acc = await_rest(l, 0)
+        tail = acc[:, hp_cols:]
+        squares = tail[:, LANES - 2 : LANES - 1] + tail[:, LANES - 1 : LANES]
+        factor = lax.rsqrt(squares / d_model + EPS)
+        proj = (acc * factor).astype(BF16).astype(F32)
+        for s in range(seqs):
+            padded[l, s, FRONT : FRONT + slots, :] = proj[s * slots : (s + 1) * slots, :hp_cols]
+        inp = convolve(padded, taps[l])
+        raw_step = proj[:, hp_cols:] + par[l, 0:1, :]
+        step = (jnp.maximum(raw_step, 0.0) + jnp.log1p(jnp.exp(-jnp.abs(raw_step)))) * mask
+        step = jnp.where(lane < heads, step, 0.0)
+        logdec = extra_rows[l] * mask - step * jnp.exp(par[l, 1:2, :])
+        logdec = jnp.where(lane < heads, logdec, 0.0)
+        parts = dot(tri, jnp.concatenate(thirds(logdec), axis=1))
+        sums = parts[:, :LANES] + parts[:, LANES : 2 * LANES] + parts[:, 2 * LANES :]
+        sums_t = sums.T
+        step_t = step.T
+        sums_parts, step_parts = thirds(sums), thirds(step)
+        both = dot(jnp.concatenate(sums_parts + step_parts, axis=0), ex)
+        sums_x = both[:rows] + both[rows : 2 * rows] + both[2 * rows : 3 * rows]
+        step_x = both[3 * rows : 4 * rows] + both[4 * rows : 5 * rows] + both[5 * rows :]
+        last_x = jnp.concatenate(
+            [
+                jnp.broadcast_to(sums_x[(s + 1) * slots - 1 : (s + 1) * slots, :], (slots, hp_cols))
+                for s in range(seqs)
+            ],
+            axis=0,
+        )
+        weighted = (jnp.exp(last_x - sums_x) * step_x * inp).astype(BF16)
+        inp_b = inp.astype(BF16)
+        grow = jnp.exp(sums_x)
+        direct = skip_x[l] * inp
+        rows_sum = sum(dot(ext, piece, 1, 1) for piece in sums_parts)
+        segs = []
+        for h in range(heads):
+            gap = sums[:, h : h + 1] - sums_t[h : h + 1, :]
+            segs.append(jnp.exp(jnp.where(causal, gap, -jnp.inf)) * step_t[h : h + 1, :])
+
+        if l == 0:
+            for k in range(1, n_tp):
+                remote(
+                    c_send.at[0], c_recv.at[k], c_ss.at[k - 1], c_rs.at[k - 1], {"tp": jnp.bitwise_xor(tp, k)}
+                ).wait_recv()
+            total = c_recv[0].astype(F32)
+            for k in range(1, n_tp):
+                total = total + c_recv[k].astype(F32)
+            mrows[...] = jnp.concatenate([total[:n_rows], total[n_rows:]], axis=1)
+            for i in range(layers):
+                for s in range(seqs):
+                    n = i * per_layer + s * keep
+                    padded_m[i, s, FRONT - keep : FRONT, :] = mrows[n : n + keep, :]
+        remote(
+            m_recv.at[l, 0 : every - 1], m_recv.at[l, 0 : every - 1], m_ss.at[l], m_rs.at[l], at(0, 1)
+        ).wait_recv()
+        got = m_recv[l].astype(F32).reshape(n_dp, n_tp, 8, LANES)
+        got = sum(got[b] for b in range(n_dp))
+        cell = over(lane, ng)
+        columns = []
+        for which in range(2):
+            blocks = []
+            for q in range(quads):
+                n = 2 * q + which
+                piece = got[0]
+                for t in range(1, n_tp):
+                    piece = jnp.where(cell == (n + t) % n_tp, got[t], piece)
+                blocks.append(piece if n == 0 else pltpu.roll(piece, LANES - ng * n, 1))
+            columns.append(jnp.concatenate(blocks, axis=0))
+        proj_m = (jnp.concatenate(columns, axis=1) * factor).astype(BF16).astype(F32)
+        for s in range(seqs):
+            padded_m[l, s, FRONT : FRONT + slots, :] = proj_m[s * slots : (s + 1) * slots]
+        n = l * per_layer + seqs * keep
+        both_maps = convolve(padded_m, mrows[n : n + taps_n, :]).astype(BF16)
+        b_map, c_map = both_maps[:, :n_state], both_maps[:, n_state:]
+        cross = dot(c_map, b_map, 1, 1)
+        within = jnp.concatenate(
+            [
+                dot((cross * segs[h]).astype(BF16), inp_b[:, h * head_size : (h + 1) * head_size])
+                for h in range(heads)
+            ],
+            axis=1,
+        )
+        carried = jnp.concatenate(
+            [
+                dot(c_map[s * slots : (s + 1) * slots], state[l, s].astype(BF16), 1, 1)
+                for s in range(seqs)
+            ],
+            axis=0,
+        )
+        acc = await_rest(l, 1)
+        later = (acc * factor).astype(BF16).astype(F32)
+        gate = later[:, :hp_cols]
+        gate = gate * jax.nn.sigmoid(gate)
+        read = (within + carried * grow + direct) * gate
+        power = read * read
+        p_hi = power.astype(BF16)
+        p_lo = (power - p_hi.astype(F32)).astype(BF16)
+        mean = (dot(p_hi, ones) + dot(p_lo, ones)) / head_size
+        headout = (read * lax.rsqrt(mean + EPS) * gain[l : l + 1, :] * mask).astype(BF16)
+        h_recv[l, 0, 0] = headout
+        own = h_recv.at[l, 0, 0]
+        targets = [(1, 0)] + [(i, k) for k in near_first for i in (0, 1)]
+        for i, k in targets:
+            remote(own, h_recv.at[l, i, k], h_ss.at[l, i, k], h_rs.at[l, i, k], at(i, k)).start()
+
+        def heads_in(i, k):
+            remote(own, h_recv.at[l, i, k], h_ss.at[l, i, k], h_rs.at[l, i, k], at(i, k)).wait_recv()
+
+        def push(k):
+            value = jnp.concatenate([h_recv[l, 0, k], h_recv[l, 1, k]], axis=1)
+            block = jnp.bitwise_xor(dp, k)
+            o_send[l, k] = dot(value, wout[l].reshape(2 * hp_cols, half)).astype(BF16)
+            for j in z_peers:
+                remote(
+                    o_send.at[l, k], o_recv.at[l, j, k], o_ss.at[l, j - 1, k], o_rs.at[l, j - 1, k],
+                    {"tp": jnp.bitwise_xor(tp, 2 * j)},
+                ).start()
+
+        if l == 0:
+            swap.wait_recv()
+        heads_in(1, 0)
+        push(0)
+        for s in range(seqs):
+            span = slice(s * slots, (s + 1) * slots)
+            fresh = dot(weighted[span], b_map[span], 0, 0)
+            end = (s + 1) * slots - 1
+            ssm[l, s] = jnp.exp(rows_sum[:, end : end + 1]) * state[l, s] + fresh
+        for k in near_first:
+            heads_in(0, k)
+            heads_in(1, k)
+            push(k)
+
+        r, c = grid(LANES, LANES)
+        own_maps = dot(later[:, hp_cols:].astype(BF16), ones_where(r == ((c + ng * tp) & (LANES - 1))))
+        own_maps = own_maps.astype(BF16)
+        r, c = grid(LANES, LANES)
+        unsort = ones_where(
+            c == (over(r, ng) & 1) * map_cols + groups * (r & (ng - 1)) + over(r, pair_cols)
+        )
+        own_maps = dot(own_maps, unsort)
+        for s in range(seqs):
+            pick = lax.broadcasted_iota(jnp.int32, (8, FRONT + slots), 0)
+            spot = lax.broadcasted_iota(jnp.int32, (8, FRONT + slots), 1)
+            chooser = ((spot == pick + lens[s] + (FRONT - keep)) & (pick < keep)).astype(BF16)
+            kept = dot(chooser, padded[l, s].astype(BF16)).astype(BF16)
+            r, c = grid(8, slots)
+            later_pick = ones_where((c == r + lens[s] - keep) & (r < keep))
+            maps_kept = dot(later_pick, own_maps[s * slots : (s + 1) * slots].astype(BF16))
+            for t in range(keep):
+                kept_u[l, t, s : s + 1, :] = kept[t : t + 1]
+                old = jnp.zeros((1, LANES), F32)
+                for n in range(keep):
+                    flat = jnp.concatenate(
+                        [cache_m[l, s, n].astype(F32)[which : which + 1] for which in range(2)], axis=1
+                    )
+                    old = jnp.where(t + lens[s] == n, flat, old)
+                line = (maps_kept[t : t + 1] + old).astype(BF16)
+                for which in range(2):
+                    kept_m[l, s, t, which : which + 1, :] = line[:, which * map_cols : (which + 1) * map_cols]
+
+        def gather(k):
+            for j in z_peers:
+                remote(
+                    o_send.at[l, k], o_recv.at[l, j, k], o_ss.at[l, j - 1, k], o_rs.at[l, j - 1, k],
+                    {"tp": jnp.bitwise_xor(tp, 2 * j)},
+                ).wait_recv()
+            o_recv[l, 0, k] = o_send[l, k]
+            block = jnp.bitwise_xor(dp, k)
+            total = o_recv[l, zed, k].astype(F32)
+            for z in range(1, n_z):
+                total = total + o_recv[l, jnp.bitwise_xor(zed, z), k].astype(F32)
+            nb[l, side, block] = total.astype(BF16)
+            remote(
+                nb.at[l, side, block], nb.at[l, side, block], n_ss.at[l, k], n_rs.at[l, k], at(1, 0)
+            ).start()
+
+        order = [0, *near_first]
+        for k in order:
+            gather(k)
+        for k in order:
+            block = jnp.bitwise_xor(dp, k)
+            remote(
+                nb.at[l, side, block], nb.at[l, 1 - side, block], n_ss.at[l, k], n_rs.at[l, k], at(1, 0)
+            ).wait_recv()
+        for h in range(2):
+            stream[:, h * half : (h + 1) * half] += nb[l, h].astype(F32).reshape(tokens, half)
+
+    for c in sends:
+        c.wait_send()
+    swap.wait_send()
+    for l in range(layers):
+        for i, j in others:
+            remote(m_send.at[l, 0, 0], m_recv.at[l, 0], m_ss.at[l], m_rs.at[l], at(i, j)).wait_send()
+        for k in dp_peers:
+            for p in range(2):
+                remote(
+                    a_send.at[l, p, 0], a_recv.at[l, p, k - 1], a_ss.at[l, p, k - 1], a_rs.at[l, p, k - 1], at(0, k)
+                ).wait_send()
+        for i, k in [(1, 0)] + [(i, k) for k in near_first for i in (0, 1)]:
+            remote(
+                h_recv.at[l, 0, 0], h_recv.at[l, i, k], h_ss.at[l, i, k], h_rs.at[l, i, k], at(i, k)
+            ).wait_send()
+        for k in range(n_dp):
+            for j in z_peers:
+                remote(
+                    o_send.at[l, k], o_recv.at[l, j, k], o_ss.at[l, j - 1, k], o_rs.at[l, j - 1, k], at(2 * j, 0)
+                ).wait_send()
+            remote(nb.at[l, 0, 0], nb.at[l, 0, 0], n_ss.at[l, k], n_rs.at[l, k], at(1, 0)).wait_send()
+
+
+def finish(stream, kept_u, kept_m, ssm, stream_out, kept_u_out, kept_m_out, ssm_out, sems):
+    pairs = ((ssm, ssm_out), (stream, stream_out), (kept_u, kept_u_out), (kept_m, kept_m_out))
+    copies = [pltpu.make_async_copy(a, b, sems.at[i]) for i, (a, b) in enumerate(pairs)]
+    for c in copies:
+        c.start()
+    for c in copies:
+        c.wait()
+
+
+def fits(n_tp, n_dp, heads, hp_cols, map_cols, n_state, rows, d_here, keep):
+    groups = map_cols * n_tp // n_state
+    powers = all(n & (n - 1) == 0 for n in (n_tp, n_dp, groups, map_cols // groups))
+    return (
+        powers and n_tp > 1 and n_dp > 1 and n_tp * n_dp <= 64 and n_tp % groups == 0 and map_cols % groups == 0
+        and hp_cols % LANES == 0 and 2 * map_cols == LANES and n_state == LANES
+        and rows * 2 * (map_cols // groups) == 8 * LANES and d_here % (2 * LANES) == 0
+        and keep <= FRONT and heads <= LANES - 2
+    )
+
+
+def body(n_tp, n_dp, *args):
+    (
+        tokens, lengths, input_norm_scale, gate_input_weight, maps_weight, step_weight,
+        input_tap_weight, map_tap_weight, step_size_bias, decay_rate_logarithm, direct_path_weight,
+        head_norm_scale, output_weight, convolution_input_cache, convolution_map_cache,
+        recurrent_state, extra_log_decay,
+    ) = args
+    layers, seqs, slots, heads = extra_log_decay.shape
+    head_size, n_state = recurrent_state.shape[3:]
+    hp_cols = heads * head_size
+    map_cols = maps_weight.shape[3]
+    rows = seqs * slots
+    d_here = tokens.shape[1]
+    keep = convolution_input_cache.shape[2]
+    if not fits(n_tp, n_dp, heads, hp_cols, map_cols, n_state, rows, d_here, keep):
+        return general_body(n_tp, n_dp, *args)
+    groups = map_cols * n_tp // n_state
+    n_z = n_tp // 2
+    taps_n = keep + 1
+    n_rows = -(-layers * (seqs * keep + taps_n) // 8) * 8
+
+    state = recurrent_state.reshape(layers, seqs, hp_cols, n_state)
+    operands = [
+        lengths, tokens, input_norm_scale, gate_input_weight,
+        jnp.transpose(maps_weight, (0, 2, 3, 1)).reshape(layers, 2 * map_cols, d_here),
+        jnp.transpose(step_weight, (0, 2, 1)),
+        input_tap_weight, map_tap_weight, step_size_bias, decay_rate_logarithm, direct_path_weight, head_norm_scale,
+        jnp.transpose(convolution_input_cache, (0, 2, 1, 3)), convolution_map_cache,
+        jnp.transpose(extra_log_decay, (0, 1, 3, 2)), state, output_weight,
+    ]
+    vmem = pl.BlockSpec(memory_space=pltpu.VMEM)
+    hbm = pl.BlockSpec(memory_space=pltpu.HBM)
+    sems = lambda *n: pltpu.SemaphoreType.DMA((layers, *n))
+    held = [pltpu.VMEM(a.shape, a.dtype) for a in operands[1:-1]]
+    held[2] = pltpu.VMEM((layers, hp_cols // LANES, d_here, 2, LANES), BF16)
+    results = (
+        jax.ShapeDtypeStruct(tokens.shape, F32),
+        jax.ShapeDtypeStruct((layers, keep, seqs, hp_cols), BF16),
+        jax.ShapeDtypeStruct((layers, seqs, keep, 2, map_cols), BF16),
+        jax.ShapeDtypeStruct(state.shape, F32),
+    )
+    made = pl.pallas_call(
+        functools.partial(
+            kernel, n_tp, n_dp, d_here * n_dp, groups,
+            (layers, seqs, slots, heads, head_size, n_state, hp_cols, map_cols),
+        ),
+        out_shape=results,
+        in_specs=[hbm] * len(operands),
+        out_specs=(vmem,) * len(results),
+        scratch_shapes=[
+            pltpu.SMEM(lengths.shape, jnp.int32),
+            *held,
+            pltpu.VMEM((layers, 2, hp_cols, d_here // 2), BF16),
+            pltpu.SemaphoreType.DMA((len(operands),)),
+            sems(hp_cols // LANES),
+            pltpu.VMEM((layers, 2, n_dp, rows, hp_cols + LANES), BF16),
+            pltpu.VMEM((layers, 2, n_dp - 1, rows, hp_cols + LANES), BF16),
+            pltpu.VMEM((layers, groups, n_dp, 8, LANES), BF16),
+            pltpu.VMEM((layers, n_dp * n_tp, 8, LANES), BF16),
+            pltpu.VMEM((groups, 2 * n_rows, LANES), BF16),
+            pltpu.VMEM((n_tp, 2 * n_rows, LANES), BF16),
+            pltpu.VMEM((layers, 2, n_dp, rows, hp_cols), BF16),
+            pltpu.VMEM((layers, n_dp, rows, d_here // 2), BF16),
+            pltpu.VMEM((layers, n_z, n_dp, rows, d_here // 2), BF16),
+            pltpu.VMEM((layers, 2, n_dp, rows, d_here // 2), BF16),
+            pltpu.VMEM((layers, seqs, FRONT + slots, hp_cols), F32),
+            pltpu.VMEM((layers, seqs, FRONT + slots, 2 * n_state), F32),
+            pltpu.VMEM((2, n_rows, LANES), F32),
+            pltpu.VMEM((n_rows, 2 * n_state), F32),
+            pltpu.VMEM((layers, LANES, d_here), BF16),
+            pltpu.VMEM((layers, LANES, d_here), BF16),
+            pltpu.VMEM((layers, 8, hp_cols), F32),
+            pltpu.VMEM((layers, 8, LANES), F32),
+            pltpu.VMEM((layers, LANES, LANES), F32),
+            sems(2, n_dp - 1), sems(2, n_dp - 1),
+            pltpu.SemaphoreType.DMA((layers,)), pltpu.SemaphoreType.DMA((layers,)),
+            pltpu.SemaphoreType.DMA((n_tp - 1,)), pltpu.SemaphoreType.DMA((n_tp - 1,)),
+            sems(2, n_dp), sems(2, n_dp),
+            sems(n_z - 1, n_dp), sems(n_z - 1, n_dp),
+            sems(n_dp), sems(n_dp),
+            pltpu.SemaphoreType.DMA, pltpu.SemaphoreType.DMA,
+        ],
+        compiler_params=pltpu.CompilerParams(
+            collective_id=0, has_side_effects=True, vmem_limit_bytes=32 * 2**20
+        ),
+        name="mixer",
+    )(*[pltpu.with_memory_space_constraint(a, pltpu.HBM) for a in operands])
+    stream, conv_in, conv_maps, ssm = pl.pallas_call(
+        finish,
+        out_shape=results,
+        in_specs=[vmem] * len(results),
+        out_specs=(hbm,) * len(results),
+        scratch_shapes=[pltpu.SemaphoreType.DMA((len(results),))],
+        compiler_params=pltpu.CompilerParams(vmem_limit_bytes=2**20),
+        name="finish",
+    )(*made)
+    return stream, jnp.transpose(conv_in, (0, 2, 1, 3)), conv_maps, ssm.reshape(recurrent_state.shape)
+
+
 def solution(mesh):
     placed = (
         P(None, "dp"),

time: 54.5 us -> 41.7 us (0.77)
  Pallas kernels: 49.1 us -> 40.9 us
  local copies, waits for them, and re-layouts: 4.4 us -> 0 us
    pallas_call x1 -> x2, Pallas kernels: 49.1 us -> 40.9 us  [the longest x1 40 us: body(): pl.pallas_call(functools.partial(kernel, n_tp, n_dp, d_here * n_dp, group...]
    reshape x2 -> x0, local copies, waits for them, and re-layouts: 2.23 us -> none  [the longest x1 1.55 us: body(): w_pair = wide(gate_input_weight.reshape(layers, 2 * d_here, hp_cols))]
    unnamed x35 -> x0, local copies, waits for them, and re-layouts: 2.16 us -> none
where the time goes in v1:
time: 41.7 us; the launch traced here: 41.5 us
  Pallas kernels  40.9 us (98%)
  between operations  0.65 us (2%)
    pallas_call x1, Pallas kernels, body(): pl.pallas_call(functools.partial(kernel, n_tp, n_dp, d_here * n_dp, group...  40 us
    pallas_call x1, Pallas kernels, body(): pl.pallas_call(finish, out_shape=results, in_specs=[vmem] * len(results),...  0.92 us

profile of v1, /device:TPU:0, one launch (start us, length us, event | category | flops | bytes accessed | tf_op | source)
XLA Modules:
  0.0 41.5 jit_solution(4148219584444543030)
XLA Ops:
  0.6 40.0 %mixer.1 = (f32[128,512]{1,0:T(8,128)S(1)}, bf16[2,3,2,256]{3,2,1,0:T(2,128)(2,1)S(1)}, bf16[2,2,3,2,64]{4,3,2,1,0:T(2,128)(2,1)S(1)}, f32[2,2,256,128]{3,2,1,0:T(8,128)S(1)}) custom-call(s32[2]{0:T(128)} %refs_0_.1, bf16[128,512]{1,0:T(8,128)(2,1)} %refs_1_.1, f32[2,512]{1,0:T(2,128)} %refs_2_.1, bf16[2,512,2,256]{3,2,1,0:T(2,128)(2,1)} %refs_3_.1, ...), custom_call_target="tpu_custom_call" | custom-call | tf_op jit(solution)/shard_map/mixer/pallas_call | solution.py:931
  40.6 0.9 %finish.1 = (f32[128,512]{1,0:T(8,128)}, bf16[2,3,2,256]{3,2,1,0:T(2,128)(2,1)}, bf16[2,2,3,2,64]{4,3,2,1,0:T(2,128)(2,1)}, f32[2,2,256,128]{3,2,1,0:T(8,128)}) custom-call(f32[128,512]{1,0:T(8,128)S(1)} %get-tuple-element.12.stream, bf16[2,3,2,256]{3,2,1,0:T(2,128)(2,1)S(1)} %get-tuple-element.13.kept_u, ...), custom_call_target="tpu_custom_call" | custom-call | tf_op jit(solution)/shard_map/finish/pallas_call | solution.py:977

commit v2 on v1

--- a/solution.py
+++ b/solution.py
@@ -420,9 +420,9 @@
         stream, kept_u, kept_m, ssm,
         lens, x, scale, w_gate, w_maps, w_step, tap_u, tap_m, bias, rate, skip, gain, cache_u, cache_m, extra_t, state,
         wout, in_sem, g_sem,
-        a_send, a_recv, m_send, m_recv, c_send, c_recv, h_recv, o_send, o_recv, nb,
-        padded, padded_m, mrow, mrows, step_w, w_sorted, taps, par, extra,
-        a_ss, a_rs, m_ss, m_rs, c_ss, c_rs, h_ss, h_rs, o_ss, o_rs, n_ss, n_rs, w_ss, w_rs,
+        t_send, t_recv, u_send, u_recv, z_send, z_recv, q_send, q_recv, m_send, m_recv, c_send, c_recv, h_recv, o_send, o_recv, nb,
+        padded, padded_m, mrow, mrows, w_rows, w_sorted, w_flat, taps, par, extra,
+        out_sem, a_rs, m_rs, c_rs, h_rs, o_rs, n_rs, w_rs, f_rs,
     ) = refs[len(names) :]
     layers, seqs, slots, heads, head_size, n_state, hp_cols, map_cols = shapes
     tp, dp = lax.axis_index("tp"), lax.axis_index("dp")
@@ -444,10 +444,13 @@
     near_first = peers(n_dp, (1, 2, 3))
     z_peers = peers(n_z, (3, 2, 1))
 
-    def remote(src, dst, ss, rs, where):
+    def remote(src, dst, arrived, where):
         return pltpu.make_async_remote_copy(
-            src_ref=src, dst_ref=dst, send_sem=ss, recv_sem=rs, device_id=where
+            src_ref=src, dst_ref=dst, send_sem=out_sem, recv_sem=arrived, device_id=where
         )
+
+    def landed(block, arrived):
+        remote(block, block, arrived, {"tp": jnp.bitwise_xor(tp, 1)}).wait_recv()
 
     barrier = pltpu.get_barrier_semaphore()
     others = [
@@ -473,7 +476,7 @@
     gate_copies = [
         [
             pltpu.make_async_copy(
-                hbm["gate"].at[l, :, :, i : i + LANES], w_gate.at[l, i // LANES], g_sem.at[l, i // LANES]
+                hbm["gate"].at[l, :, :, i : i + LANES], w_gate.at[l, i // LANES], g_sem.at[l]
             )
             for i in range(0, hp_cols, LANES)
         ]
@@ -499,17 +502,27 @@
     wanted = (over(place, ng) & 1) * map_cols + groups * (place & (ng - 1)) + over(place, pair_cols)
     sorter = ones_where(r == wanted)
     home = over((lane + LANES - ng * tp) & (LANES - 1), pair_cols)
-    step_w[...] = jnp.zeros_like(step_w)
+    for l in range(layers):
+        w_rows[l, :LANES] = jnp.zeros_like(w_rows[l, :LANES])
     gate_rows = w_gate.reshape(layers, hp_cols // LANES, 2 * d_here, LANES)
 
     def group_of(rank):
         return rank * groups // n_tp
 
-    def project(l):
+    def start_of(l):
         st = stream[...]
         squares = jnp.sum(st * st, axis=1, keepdims=True)
-        normed = (st * scale[l : l + 1, :]).astype(BF16)
-        raw = dot(normed, w_sorted[l], 1, 1)
+        return (st * scale[l : l + 1, :]).astype(BF16), squares
+
+    def with_squares(tail, squares):
+        high = squares.astype(BF16).astype(F32)
+        return jnp.where(lane == LANES - 2, high, jnp.where(lane == LANES - 1, squares - high, tail))
+
+    def fill(buffer, l, value):
+        for b in range(n_dp):
+            buffer[l, b, :, : value.shape[1]] = value[b * rows : (b + 1) * rows].astype(BF16)
+
+    def pack_maps(l, raw):
         turned = [raw if k == 0 else pltpu.roll(raw, k * pair_cols, 1) for k in range(quads)]
         turned = [t.reshape(n_dp, quads, 8, LANES) for t in turned]
         for g in range(groups):
@@ -517,79 +530,108 @@
             for q in range(1, quads):
                 piece = jnp.where((home == q)[None], turned[(q - g) % quads][:, q], piece)
             m_send[l, g] = piece.astype(BF16)
-        return normed, squares, raw
 
     def send_maps(l):
         for i, j in others:
             to = at(i, j)
             remote(
-                m_send.at[l, group_of(to["tp"]), to["dp"]], m_recv.at[l, me], m_ss.at[l], m_rs.at[l], to
+                m_send.at[l, group_of(to["tp"]), to["dp"]], m_recv.at[l, me], m_rs, to
             ).start()
         m_recv[l, me] = m_send[l, group_of(tp), dp]
 
-    def project_rest(l, normed, squares, raw):
-        spreads = [dot(normed[:, i : i + LANES], spread).astype(BF16) for i in range(0, d_here, LANES)]
-        even = jnp.concatenate([s[:, : 2 * LANES] for s in spreads], axis=1)
-        odd = jnp.concatenate([s[:, 2 * LANES :] for s in spreads], axis=1)
-        for c in gate_copies[l]:
-            c.wait()
-        weight = jnp.concatenate([gate_rows[l, i] for i in range(hp_cols // LANES)], axis=1)
-        both = dot(jnp.concatenate([odd, even], axis=0), weight)
-        tail = dot(normed, step_w[l], 1, 1)
-        high = squares.astype(BF16).astype(F32)
-        tail = jnp.where(lane == LANES - 2, high, jnp.where(lane == LANES - 1, squares - high, tail))
-        one = jnp.concatenate([both[:tokens], tail], axis=1).astype(BF16)
-        two = jnp.concatenate([both[tokens:], raw], axis=1).astype(BF16)
-        for b in range(n_dp):
-            a_send[l, 0, b] = one[b * rows : (b + 1) * rows]
-            a_send[l, 1, b] = two[b * rows : (b + 1) * rows]
-
-    def send_rest(l):
-        for p in range(2):
-            for k in dp_peers:
-                to = jnp.bitwise_xor(dp, k)
-                remote(
-                    a_send.at[l, p, to], a_recv.at[l, p, k - 1], a_ss.at[l, p, k - 1], a_rs.at[l, p, k - 1], {"dp": to}
-                ).start()
-
-    def await_rest(l, p):
-        acc = a_send[l, p, dp].astype(F32)
+    def rows_of(rank, which):
+        return pl.ds(pl.multiple_of(LANES + which * n_state + ng * rank, ng), ng)
+
+    def pick_rows(rank, which):
+        return pl.ds(pl.multiple_of(pair_cols * group_of(rank) + which * ng, ng), ng)
+
+    def fetch(i, k, which):
+        to = jnp.bitwise_xor(tp, k)
+        n = 2 * (i - 1) + (k == 1)
+        return remote(
+            w_sorted.at[i, pick_rows(to, which)], w_rows.at[i, rows_of(tp, which)], f_rs.at[n], {"tp": to}
+        )
+
+    def relay(i, j, which):
+        n = 2 * (i - 1) + 1
+        block = w_rows.at[i, rows_of(jnp.bitwise_xor(tp, 2 * j), which)]
+        return remote(block, block, f_rs.at[n], at(1, 0))
+
+    def fetched(i, far):
+        n = 2 * (i - 1) + 1 - far
+        landed(w_rows.at[i, pl.ds(LANES, 2 * ng * (n_z - 1 if far else n_z))], f_rs.at[n])
+
+    parts_of = ((t_send, t_recv), (u_send, u_recv), (z_send, z_recv), (q_send, q_recv))
+
+    def part(l, p, k):
+        send, recv = parts_of[p]
+        to = jnp.bitwise_xor(dp, k)
+        src, dst = send.at[l, to], recv.at[l, k - 1]
+        if p == 0 and l == 0:
+            src, dst = src.at[:, :LANES], dst.at[:, :LANES]
+        return remote(src, dst, a_rs.at[l, p], {"dp": to})
+
+    def send_part(l, p):
         for k in dp_peers:
-            remote(
-                a_send.at[l, p, 0], a_recv.at[l, p, k - 1], a_ss.at[l, p, k - 1], a_rs.at[l, p, k - 1],
-                {"dp": jnp.bitwise_xor(dp, k)},
-            ).wait_recv()
+            part(l, p, k).start()
+
+    def await_part(l, p):
+        send, recv = parts_of[p]
+        width = LANES if p == 0 and l == 0 else send.shape[-1]
+        landed(recv.at[l, :, :, :width], a_rs.at[l, p])
+        acc = send[l, dp, :, :width].astype(F32)
         for k in range(1, n_dp):
-            acc = acc + a_recv[l, p, k - 1].astype(F32)
+            acc = acc + recv[l, k - 1, :, :width].astype(F32)
         return acc
+
+    def flat_weight(l):
+        return jnp.concatenate([gate_rows[l, i] for i in range(hp_cols // LANES)], axis=1)
 
     sends = []
     for name in first:
         local[name].wait()
     for l in range(layers):
-        step_w[l, :heads, :] = w_step[l]
+        w_rows[l, :heads, :] = w_step[l]
     w_sorted[0] = dot(sorter, w_maps[0], 0, 0).astype(BF16)
     stream[...] = x[...].astype(F32)
 
     for l in range(layers):
-        normed, squares, raw = project(l)
+        normed, squares = start_of(l)
         if l == 0:
-            project_rest(l, normed, squares, raw)
+            raw = dot(normed, w_sorted[l], 1, 1)
+            pack_maps(l, raw)
+            fill(t_send, l, with_squares(dot(normed, w_rows[l, :LANES], 1, 1), squares))
+            spreads = [dot(normed[:, i : i + LANES], spread).astype(BF16) for i in range(0, d_here, LANES)]
+            even = jnp.concatenate([s[:, : 2 * LANES] for s in spreads], axis=1)
+            odd = jnp.concatenate([s[:, 2 * LANES :] for s in spreads], axis=1)
+            pltpu.make_async_copy(w_gate.at[l], w_gate.at[l], g_sem.at[l]).wait()
+            both = dot(jnp.concatenate([odd, even], axis=0), flat_weight(l))
+            fill(u_send, l, both[:tokens])
+            fill(z_send, l, both[tokens:])
+            fill(q_send, l, raw)
             pl.semaphore_wait(barrier, every - 1)
-        send_maps(l)
-        if l > 0:
-            project_rest(l, normed, squares, raw)
-        send_rest(l)
+            send_maps(l)
+            for p in range(4):
+                send_part(l, p)
+        else:
+            fetched(l, 0)
+            tail = dot(normed, w_rows[l], 1, 1)
+            fill(t_send, l, jnp.concatenate([with_squares(tail[:, :LANES], squares), tail[:, LANES:]], axis=1))
+            send_part(l, 0)
+            fill(u_send, l, dot(normed, w_flat[l - 1, 1]))
+            send_part(l, 1)
+            fill(z_send, l, dot(normed, w_flat[l - 1, 0]))
+            send_part(l, 2)
+            fill(q_send, l, dot(normed, w_sorted[l], 1, 1))
+            send_part(l, 3)
 
         if l == 0:
             for n in range(len(pairs) + 1):
                 name = [*pairs, "wout"][n]
                 if name not in first:
                     local[name].wait()
-            swap = remote(hbm["wout"].at[:, :, theirs], wout.at[:, 1], w_ss, w_rs, {"tp": jnp.bitwise_xor(tp, 1)})
+            swap = remote(hbm["wout"].at[:, :, theirs], wout.at[:, 1], w_rs, {"tp": jnp.bitwise_xor(tp, 1)})
             swap.start()
-            for i in range(1, layers):
-                w_sorted[i] = dot(sorter, w_maps[i], 0, 0).astype(BF16)
             per_layer = seqs * keep + taps_n
             mrow[...] = jnp.zeros_like(mrow)
             for i in range(layers):
@@ -613,10 +655,14 @@
                 c_send[g] = packed[:, g * LANES : (g + 1) * LANES]
             for k in peers(n_tp, (6, 7, 4, 5, 2, 3, 1)):
                 to = jnp.bitwise_xor(tp, k)
-                c = remote(c_send.at[group_of(to)], c_recv.at[k], c_ss.at[k - 1], c_rs.at[k - 1], {"tp": to})
+                c = remote(c_send.at[group_of(to)], c_recv.at[k], c_rs, {"tp": to})
                 c.start()
                 sends.append(c)
             c_recv[0] = c_send[group_of(tp)]
+            r, c = grid(LANES, LANES)
+            resort = ones_where(r == (over(c, ng) & 1) * map_cols + groups * (c & (ng - 1)) + over(c, pair_cols))
+            for i in range(1, layers):
+                w_sorted[i] = dot(resort, w_maps[i], 0, 0).astype(BF16)
 
             slot = lax.broadcasted_iota(jnp.int32, (slots, 1), 0)
             mask = jnp.concatenate([(slot < lens[s]).astype(F32) for s in range(seqs)], axis=0)
@@ -658,15 +704,11 @@
             out = jnp.concatenate(pieces, axis=0)
             return out * jax.nn.sigmoid(out)
 
-        acc = await_rest(l, 0)
-        tail = acc[:, hp_cols:]
+        acc = await_part(l, 0)
+        tail = acc[:, :LANES]
         squares = tail[:, LANES - 2 : LANES - 1] + tail[:, LANES - 1 : LANES]
         factor = lax.rsqrt(squares / d_model + EPS)
-        proj = (acc * factor).astype(BF16).astype(F32)
-        for s in range(seqs):
-            padded[l, s, FRONT : FRONT + slots, :] = proj[s * slots : (s + 1) * slots, :hp_cols]
-        inp = convolve(padded, taps[l])
-        raw_step = proj[:, hp_cols:] + par[l, 0:1, :]
+        raw_step = (tail * factor).astype(BF16).astype(F32) + par[l, 0:1, :]
         step = (jnp.maximum(raw_step, 0.0) + jnp.log1p(jnp.exp(-jnp.abs(raw_step)))) * mask
         step = jnp.where(lane < heads, step, 0.0)
         logdec = extra_rows[l] * mask - step * jnp.exp(par[l, 1:2, :])
@@ -679,28 +721,54 @@
         both = dot(jnp.concatenate(sums_parts + step_parts, axis=0), ex)
         sums_x = both[:rows] + both[rows : 2 * rows] + both[2 * rows : 3 * rows]
         step_x = both[3 * rows : 4 * rows] + both[4 * rows : 5 * rows] + both[5 * rows :]
-        last_x = jnp.concatenate(
-            [
-                jnp.broadcast_to(sums_x[(s + 1) * slots - 1 : (s + 1) * slots, :], (slots, hp_cols))
-                for s in range(seqs)
-            ],
-            axis=0,
-        )
-        weighted = (jnp.exp(last_x - sums_x) * step_x * inp).astype(BF16)
-        inp_b = inp.astype(BF16)
         grow = jnp.exp(sums_x)
-        direct = skip_x[l] * inp
-        rows_sum = sum(dot(ext, piece, 1, 1) for piece in sums_parts)
         segs = []
         for h in range(heads):
             gap = sums[:, h : h + 1] - sums_t[h : h + 1, :]
             segs.append(jnp.exp(jnp.where(causal, gap, -jnp.inf)) * step_t[h : h + 1, :])
 
+        def filter_inputs():
+            proj = (await_part(l, 1) * factor).astype(BF16).astype(F32)
+            for s in range(seqs):
+                padded[l, s, FRONT : FRONT + slots, :] = proj[s * slots : (s + 1) * slots]
+            return convolve(padded, taps[l])
+
+        def unpack_maps():
+            landed(m_recv.at[l, 0 : every - 1], m_rs)
+            got = m_recv[l].astype(F32).reshape(n_dp, n_tp, 8, LANES)
+            got = sum(got[b] for b in range(n_dp))
+            cell = over(lane, ng)
+            columns = []
+            for which in range(2):
+                blocks = []
+                for q in range(quads):
+                    n = 2 * q + which
+                    piece = got[0]
+                    for t in range(1, n_tp):
+                        piece = jnp.where(cell == (n + t) % n_tp, got[t], piece)
+                    blocks.append(piece if n == 0 else pltpu.roll(piece, LANES - ng * n, 1))
+                columns.append(jnp.concatenate(blocks, axis=0))
+            return jnp.concatenate(columns, axis=1)
+
+        def filter_maps(raw):
+            proj = (raw * factor).astype(BF16).astype(F32)
+            for s in range(seqs):
+                padded_m[l, s, FRONT : FRONT + slots, :] = proj[s * slots : (s + 1) * slots]
+            n = l * per_layer + seqs * keep
+            maps = convolve(padded_m, mrows[n : n + taps_n, :]).astype(BF16)
+            b_map, c_map = maps[:, :n_state], maps[:, n_state:]
+            carried = jnp.concatenate(
+                [
+                    dot(c_map[s * slots : (s + 1) * slots], state[l, s].astype(BF16), 1, 1)
+                    for s in range(seqs)
+                ],
+                axis=0,
+            )
+            return b_map, dot(c_map, b_map, 1, 1), carried * grow
+
         if l == 0:
-            for k in range(1, n_tp):
-                remote(
-                    c_send.at[0], c_recv.at[k], c_ss.at[k - 1], c_rs.at[k - 1], {"tp": jnp.bitwise_xor(tp, k)}
-                ).wait_recv()
+            inp = filter_inputs()
+            landed(c_recv.at[1:n_tp], c_rs)
             total = c_recv[0].astype(F32)
             for k in range(1, n_tp):
                 total = total + c_recv[k].astype(F32)
@@ -709,29 +777,18 @@
                 for s in range(seqs):
                     n = i * per_layer + s * keep
                     padded_m[i, s, FRONT - keep : FRONT, :] = mrows[n : n + keep, :]
-        remote(
-            m_recv.at[l, 0 : every - 1], m_recv.at[l, 0 : every - 1], m_ss.at[l], m_rs.at[l], at(0, 1)
-        ).wait_recv()
-        got = m_recv[l].astype(F32).reshape(n_dp, n_tp, 8, LANES)
-        got = sum(got[b] for b in range(n_dp))
-        cell = over(lane, ng)
-        columns = []
-        for which in range(2):
-            blocks = []
-            for q in range(quads):
-                n = 2 * q + which
-                piece = got[0]
-                for t in range(1, n_tp):
-                    piece = jnp.where(cell == (n + t) % n_tp, got[t], piece)
-                blocks.append(piece if n == 0 else pltpu.roll(piece, LANES - ng * n, 1))
-            columns.append(jnp.concatenate(blocks, axis=0))
-        proj_m = (jnp.concatenate(columns, axis=1) * factor).astype(BF16).astype(F32)
-        for s in range(seqs):
-            padded_m[l, s, FRONT : FRONT + slots, :] = proj_m[s * slots : (s + 1) * slots]
-        n = l * per_layer + seqs * keep
-        both_maps = convolve(padded_m, mrows[n : n + taps_n, :]).astype(BF16)
-        b_map, c_map = both_maps[:, :n_state], both_maps[:, n_state:]
-        cross = dot(c_map, b_map, 1, 1)
+            raw = unpack_maps()
+            for i in range(1, layers):
+                for k in [*[2 * j for j in z_peers], 1]:
+                    for which in range(2):
+                        fetch(i, k, which).start()
+                for which in range(2):
+                    w_rows[i, rows_of(tp, which), :] = w_sorted[i, pick_rows(tp, which), :]
+            b_map, cross, carried = filter_maps(raw)
+        else:
+            b_map, cross, carried = filter_maps(acc[:, LANES:])
+            inp = filter_inputs()
+        inp_b = inp.astype(BF16)
         within = jnp.concatenate(
             [
                 dot((cross * segs[h]).astype(BF16), inp_b[:, h * head_size : (h + 1) * head_size])
@@ -739,18 +796,11 @@
             ],
             axis=1,
         )
-        carried = jnp.concatenate(
-            [
-                dot(c_map[s * slots : (s + 1) * slots], state[l, s].astype(BF16), 1, 1)
-                for s in range(seqs)
-            ],
-            axis=0,
-        )
-        acc = await_rest(l, 1)
-        later = (acc * factor).astype(BF16).astype(F32)
-        gate = later[:, :hp_cols]
+        inner = within + carried + skip_x[l] * inp
+        acc = await_part(l, 2)
+        gate = (acc * factor).astype(BF16).astype(F32)
         gate = gate * jax.nn.sigmoid(gate)
-        read = (within + carried * grow + direct) * gate
+        read = inner * gate
         power = read * read
         p_hi = power.astype(BF16)
         p_lo = (power - p_hi.astype(F32)).astype(BF16)
@@ -760,10 +810,7 @@
         own = h_recv.at[l, 0, 0]
         targets = [(1, 0)] + [(i, k) for k in near_first for i in (0, 1)]
         for i, k in targets:
-            remote(own, h_recv.at[l, i, k], h_ss.at[l, i, k], h_rs.at[l, i, k], at(i, k)).start()
-
-        def heads_in(i, k):
-            remote(own, h_recv.at[l, i, k], h_ss.at[l, i, k], h_rs.at[l, i, k], at(i, k)).wait_recv()
+            remote(own, h_recv.at[l, i, k], h_rs.at[l, k], at(i, k)).start()
 
         def push(k):
             value = jnp.concatenate([h_recv[l, 0, k], h_recv[l, 1, k]], axis=1)
@@ -771,32 +818,47 @@
             o_send[l, k] = dot(value, wout[l].reshape(2 * hp_cols, half)).astype(BF16)
             for j in z_peers:
                 remote(
-                    o_send.at[l, k], o_recv.at[l, j, k], o_ss.at[l, j - 1, k], o_rs.at[l, j - 1, k],
+                    o_send.at[l, k], o_recv.at[l, j, k], o_rs.at[l, k],
                     {"tp": jnp.bitwise_xor(tp, 2 * j)},
                 ).start()
 
         if l == 0:
             swap.wait_recv()
-        heads_in(1, 0)
+        landed(h_recv.at[l, 1, 0], h_rs.at[l, 0])
         push(0)
+        last_x = jnp.concatenate(
+            [
+                jnp.broadcast_to(sums_x[(s + 1) * slots - 1 : (s + 1) * slots, :], (slots, hp_cols))
+                for s in range(seqs)
+            ],
+            axis=0,
+        )
+        weighted = (jnp.exp(last_x - sums_x) * step_x * inp).astype(BF16)
+        rows_sum = sum(dot(ext, piece, 1, 1) for piece in sums_parts)
         for s in range(seqs):
             span = slice(s * slots, (s + 1) * slots)
             fresh = dot(weighted[span], b_map[span], 0, 0)
             end = (s + 1) * slots - 1
             ssm[l, s] = jnp.exp(rows_sum[:, end : end + 1]) * state[l, s] + fresh
+        if l + 1 < layers:
+            pltpu.make_async_copy(w_gate.at[l + 1], w_gate.at[l + 1], g_sem.at[l + 1]).wait()
+            weight = flat_weight(l + 1)
+            r, c = grid(LANES, 2 * LANES)
+            for which in range(2):
+                picker = ones_where(c == 2 * r + which)
+                for n in range(0, d_here, LANES):
+                    w_flat[l, which, n : n + LANES] = dot(picker, weight[2 * n : 2 * (n + LANES)]).astype(BF16)
         for k in near_first:
-            heads_in(0, k)
-            heads_in(1, k)
+            landed(h_recv.at[l, :, k], h_rs.at[l, k])
             push(k)
 
         r, c = grid(LANES, LANES)
-        own_maps = dot(later[:, hp_cols:].astype(BF16), ones_where(r == ((c + ng * tp) & (LANES - 1))))
-        own_maps = own_maps.astype(BF16)
-        r, c = grid(LANES, LANES)
+        if l == 0:
+            r = (r + LANES - ng * tp) & (LANES - 1)
         unsort = ones_where(
             c == (over(r, ng) & 1) * map_cols + groups * (r & (ng - 1)) + over(r, pair_cols)
         )
-        own_maps = dot(own_maps, unsort)
+        own_maps = dot((await_part(l, 3) * factor).astype(BF16), unsort)
         for s in range(seqs):
             pick = lax.broadcasted_iota(jnp.int32, (8, FRONT + slots), 0)
             spot = lax.broadcasted_iota(jnp.int32, (8, FRONT + slots), 1)
@@ -818,11 +880,7 @@
                     kept_m[l, s, t, which : which + 1, :] = line[:, which * map_cols : (which + 1) * map_cols]
 
         def gather(k):
-            for j in z_peers:
-                remote(
-                    o_send.at[l, k], o_recv.at[l, j, k], o_ss.at[l, j - 1, k], o_rs.at[l, j - 1, k],
-                    {"tp": jnp.bitwise_xor(tp, 2 * j)},
-                ).wait_recv()
+            landed(o_recv.at[l, 1:n_z, k], o_rs.at[l, k])
             o_recv[l, 0, k] = o_send[l, k]
             block = jnp.bitwise_xor(dp, k)
             total = o_recv[l, zed, k].astype(F32)
@@ -830,17 +888,19 @@
                 total = total + o_recv[l, jnp.bitwise_xor(zed, z), k].astype(F32)
             nb[l, side, block] = total.astype(BF16)
             remote(
-                nb.at[l, side, block], nb.at[l, side, block], n_ss.at[l, k], n_rs.at[l, k], at(1, 0)
+                nb.at[l, side, block], nb.at[l, side, block], n_rs.at[l], at(1, 0)
             ).start()
 
+        if l == 0:
+            for i in range(1, layers):
+                fetched(i, 1)
+                for j in z_peers:
+                    for which in range(2):
+                        relay(i, j, which).start()
         order = [0, *near_first]
         for k in order:
             gather(k)
-        for k in order:
-            block = jnp.bitwise_xor(dp, k)
-            remote(
-                nb.at[l, side, block], nb.at[l, 1 - side, block], n_ss.at[l, k], n_rs.at[l, k], at(1, 0)
-            ).wait_recv()
+        landed(nb.at[l, 1 - side], n_rs.at[l])
         for h in range(2):
             stream[:, h * half : (h + 1) * half] += nb[l, h].astype(F32).reshape(tokens, half)
 
@@ -848,23 +908,28 @@
         c.wait_send()
     swap.wait_send()
     for l in range(layers):
-        for i, j in others:
-            remote(m_send.at[l, 0, 0], m_recv.at[l, 0], m_ss.at[l], m_rs.at[l], at(i, j)).wait_send()
+        if l == 0:
+            for i, j in others:
+                remote(m_send.at[l, 0, 0], m_recv.at[l, 0], m_rs, at(i, j)).wait_send()
+        else:
+            for which in range(2):
+                for k in [*[2 * j for j in z_peers], 1]:
+                    fetch(l, k, which).wait_send()
+                for j in z_peers:
+                    relay(l, j, which).wait_send()
         for k in dp_peers:
-            for p in range(2):
-                remote(
-                    a_send.at[l, p, 0], a_recv.at[l, p, k - 1], a_ss.at[l, p, k - 1], a_rs.at[l, p, k - 1], at(0, k)
-                ).wait_send()
+            for p in range(4):
+                part(l, p, k).wait_send()
         for i, k in [(1, 0)] + [(i, k) for k in near_first for i in (0, 1)]:
             remote(
-                h_recv.at[l, 0, 0], h_recv.at[l, i, k], h_ss.at[l, i, k], h_rs.at[l, i, k], at(i, k)
+                h_recv.at[l, 0, 0], h_recv.at[l, i, k], h_rs.at[l, k], at(i, k)
             ).wait_send()
         for k in range(n_dp):
             for j in z_peers:
                 remote(
-                    o_send.at[l, k], o_recv.at[l, j, k], o_ss.at[l, j - 1, k], o_rs.at[l, j - 1, k], at(2 * j, 0)
+                    o_send.at[l, k], o_recv.at[l, j, k], o_rs.at[l, k], at(2 * j, 0)
                 ).wait_send()
-            remote(nb.at[l, 0, 0], nb.at[l, 0, 0], n_ss.at[l, k], n_rs.at[l, k], at(1, 0)).wait_send()
+            remote(nb.at[l, 0, 0], nb.at[l, 0, 0], n_rs.at[l], at(1, 0)).wait_send()
 
 
 def finish(stream, kept_u, kept_m, ssm, stream_out, kept_u_out, kept_m_out, ssm_out, sems):
@@ -941,9 +1006,12 @@
             *held,
             pltpu.VMEM((layers, 2, hp_cols, d_here // 2), BF16),
             pltpu.SemaphoreType.DMA((len(operands),)),
-            sems(hp_cols // LANES),
-            pltpu.VMEM((layers, 2, n_dp, rows, hp_cols + LANES), BF16),
-            pltpu.VMEM((layers, 2, n_dp - 1, rows, hp_cols + LANES), BF16),
+            sems(),
+            *[
+                pltpu.VMEM((layers, n, rows, width), BF16)
+                for width in (LANES + 2 * n_state, hp_cols, hp_cols, LANES)
+                for n in (n_dp, n_dp - 1)
+            ],
             pltpu.VMEM((layers, groups, n_dp, 8, LANES), BF16),
             pltpu.VMEM((layers, n_dp * n_tp, 8, LANES), BF16),
             pltpu.VMEM((groups, 2 * n_rows, LANES), BF16),
@@ -956,18 +1024,21 @@
             pltpu.VMEM((layers, seqs, FRONT + slots, 2 * n_state), F32),
             pltpu.VMEM((2, n_rows, LANES), F32),
             pltpu.VMEM((n_rows, 2 * n_state), F32),
+            pltpu.VMEM((layers, LANES + 2 * n_state, d_here), BF16),
             pltpu.VMEM((layers, LANES, d_here), BF16),
-            pltpu.VMEM((layers, LANES, d_here), BF16),
+            pltpu.VMEM((max(layers - 1, 1), 2, d_here, hp_cols), BF16),
             pltpu.VMEM((layers, 8, hp_cols), F32),
             pltpu.VMEM((layers, 8, LANES), F32),
             pltpu.VMEM((layers, LANES, LANES), F32),
-            sems(2, n_dp - 1), sems(2, n_dp - 1),
-            pltpu.SemaphoreType.DMA((layers,)), pltpu.SemaphoreType.DMA((layers,)),
-            pltpu.SemaphoreType.DMA((n_tp - 1,)), pltpu.SemaphoreType.DMA((n_tp - 1,)),
-            sems(2, n_dp), sems(2, n_dp),
-            sems(n_z - 1, n_dp), sems(n_z - 1, n_dp),
-            sems(n_dp), sems(n_dp),
-            pltpu.SemaphoreType.DMA, pltpu.SemaphoreType.DMA,
+            pltpu.SemaphoreType.DMA,
+            sems(4),
+            pltpu.SemaphoreType.DMA,
+            pltpu.SemaphoreType.DMA,
+            sems(n_dp),
+            sems(n_dp),
+            sems(),
+            pltpu.SemaphoreType.DMA,
+            pltpu.SemaphoreType.DMA((2 * max(layers - 1, 1),)),
         ],
         compiler_params=pltpu.CompilerParams(
             collective_id=0, has_side_effects=True, vmem_limit_bytes=32 * 2**20

time: 41.7 us -> 40.3 us (0.966)
  Pallas kernels: 40.9 us -> 39.5 us
    pallas_call x1, Pallas kernels: 40 us -> 38.6 us  [body(): pl.pallas_call(functools.partial(kernel, n_tp, n_dp, d_here * n_dp, group...]
where the time goes in v2:
time: 40.3 us; the launch traced here: 40.2 us
  Pallas kernels  39.5 us (98%)
  between operations  0.65 us (2%)
    pallas_call x1, Pallas kernels, body(): pl.pallas_call(functools.partial(kernel, n_tp, n_dp, d_here * n_dp, group...  38.6 us
    pallas_call x1, Pallas kernels, body(): pl.pallas_call(finish, out_shape=results, in_specs=[vmem] * len(results),...  0.92 us

profile of v2, /device:TPU:0, one launch (start us, length us, event | category | flops | bytes accessed | tf_op | source)
XLA Modules:
  0.0 40.2 jit_solution(8214560745961705566)
XLA Ops:
  0.6 38.6 %mixer.1 = (f32[128,512]{1,0:T(8,128)S(1)}, bf16[2,3,2,256]{3,2,1,0:T(2,128)(2,1)S(1)}, bf16[2,2,3,2,64]{4,3,2,1,0:T(2,128)(2,1)S(1)}, f32[2,2,256,128]{3,2,1,0:T(8,128)S(1)}) custom-call(s32[2]{0:T(128)} %refs_0_.1, bf16[128,512]{1,0:T(8,128)(2,1)} %refs_1_.1, f32[2,512]{1,0:T(2,128)} %refs_2_.1, bf16[2,512,2,256]{3,2,1,0:T(2,128)(2,1)} %refs_3_.1, ...), custom_call_target="tpu_custom_call" | custom-call | tf_op jit(solution)/shard_map/mixer/pallas_call | solution.py:996
  39.3 0.9 %finish.1 = (f32[128,512]{1,0:T(8,128)}, bf16[2,3,2,256]{3,2,1,0:T(2,128)(2,1)}, bf16[2,2,3,2,64]{4,3,2,1,0:T(2,128)(2,1)}, f32[2,2,256,128]{3,2,1,0:T(8,128)}) custom-call(f32[128,512]{1,0:T(8,128)S(1)} %get-tuple-element.12.stream, bf16[2,3,2,256]{3,2,1,0:T(2,128)(2,1)S(1)} %get-tuple-element.13.kept_u, ...), custom_call_target="tpu_custom_call" | custom-call | tf_op jit(solution)/shard_map/finish/pallas_call | solution.py:1048

commit v3 on v2

--- a/solution.py
+++ b/solution.py
@@ -441,7 +441,7 @@
     every = n_tp * n_dp
     me = dp * n_tp + tp
     dp_peers = peers(n_dp, (3, 1, 2))
-    near_first = peers(n_dp, (1, 2, 3))
+    turns = peers(n_dp, (1, 2, 3))
     z_peers = peers(n_z, (3, 2, 1))
 
     def remote(src, dst, arrived, where):
@@ -509,11 +509,6 @@
     def group_of(rank):
         return rank * groups // n_tp
 
-    def start_of(l):
-        st = stream[...]
-        squares = jnp.sum(st * st, axis=1, keepdims=True)
-        return (st * scale[l : l + 1, :]).astype(BF16), squares
-
     def with_squares(tail, squares):
         high = squares.astype(BF16).astype(F32)
         return jnp.where(lane == LANES - 2, high, jnp.where(lane == LANES - 1, squares - high, tail))
@@ -596,8 +591,10 @@
     stream[...] = x[...].astype(F32)
 
     for l in range(layers):
-        normed, squares = start_of(l)
         if l == 0:
+            st = stream[...]
+            squares = jnp.sum(st * st, axis=1, keepdims=True)
+            normed = (st * scale[l : l + 1, :]).astype(BF16)
             raw = dot(normed, w_sorted[l], 1, 1)
             pack_maps(l, raw)
             fill(t_send, l, with_squares(dot(normed, w_rows[l, :LANES], 1, 1), squares))
@@ -613,17 +610,6 @@
             send_maps(l)
             for p in range(4):
                 send_part(l, p)
-        else:
-            fetched(l, 0)
-            tail = dot(normed, w_rows[l], 1, 1)
-            fill(t_send, l, jnp.concatenate([with_squares(tail[:, :LANES], squares), tail[:, LANES:]], axis=1))
-            send_part(l, 0)
-            fill(u_send, l, dot(normed, w_flat[l - 1, 1]))
-            send_part(l, 1)
-            fill(z_send, l, dot(normed, w_flat[l - 1, 0]))
-            send_part(l, 2)
-            fill(q_send, l, dot(normed, w_sorted[l], 1, 1))
-            send_part(l, 3)
 
         if l == 0:
             for n in range(len(pairs) + 1):
@@ -808,7 +794,7 @@
         headout = (read * lax.rsqrt(mean + EPS) * gain[l : l + 1, :] * mask).astype(BF16)
         h_recv[l, 0, 0] = headout
         own = h_recv.at[l, 0, 0]
-        targets = [(1, 0)] + [(i, k) for k in near_first for i in (0, 1)]
+        targets = [(1, 0)] + [(i, k) for k in turns for i in (0, 1)]
         for i, k in targets:
             remote(own, h_recv.at[l, i, k], h_rs.at[l, k], at(i, k)).start()
 
@@ -848,7 +834,7 @@
                 picker = ones_where(c == 2 * r + which)
                 for n in range(0, d_here, LANES):
                     w_flat[l, which, n : n + LANES] = dot(picker, weight[2 * n : 2 * (n + LANES)]).astype(BF16)
-        for k in near_first:
+        for k in turns:
             landed(h_recv.at[l, :, k], h_rs.at[l, k])
             push(k)
 
@@ -888,7 +874,7 @@
                 total = total + o_recv[l, jnp.bitwise_xor(zed, z), k].astype(F32)
             nb[l, side, block] = total.astype(BF16)
             remote(
-                nb.at[l, side, block], nb.at[l, side, block], n_rs.at[l], at(1, 0)
+                nb.at[l, side, block], nb.at[l, side, block], n_rs.at[l, k], at(1, 0)
             ).start()
 
         if l == 0:
@@ -897,12 +883,40 @@
                 for j in z_peers:
                     for which in range(2):
                         relay(i, j, which).start()
-        order = [0, *near_first]
-        for k in order:
-            gather(k)
-        landed(nb.at[l, 1 - side], n_rs.at[l])
-        for h in range(2):
-            stream[:, h * half : (h + 1) * half] += nb[l, h].astype(F32).reshape(tokens, half)
+        def receive(k):
+            landed(nb.at[l, 1 - side, jnp.bitwise_xor(dp, k)], n_rs.at[l, k])
+            block = jnp.bitwise_xor(dp, k)
+            span = pl.ds(pl.multiple_of(block * rows, rows), rows)
+            st = stream[span, :] + jnp.concatenate([nb[l, h, block].astype(F32) for h in range(2)], axis=1)
+            stream[span, :] = st
+            n = l + 1
+            if n == layers:
+                return
+            squares = jnp.sum(st * st, axis=1, keepdims=True)
+            normed = (st * scale[n : n + 1, :]).astype(BF16)
+            tail = dot(normed, w_rows[n], 1, 1)
+            tail = jnp.concatenate([with_squares(tail[:, :LANES], squares), tail[:, LANES:]], axis=1)
+            t_send[n, block] = tail.astype(BF16)
+            if k:
+                part(n, 0, k).start()
+            u_send[n, block] = dot(normed, w_flat[l, 1]).astype(BF16)
+            if k:
+                part(n, 1, k).start()
+            z_send[n, block] = dot(normed, w_flat[l, 0]).astype(BF16)
+            if k:
+                part(n, 2, k).start()
+            q_send[n, block] = dot(normed, w_sorted[n], 1, 1).astype(BF16)
+            if k:
+                part(n, 3, k).start()
+
+        order = [0, *turns]
+        gather(order[0])
+        for n in range(1, len(order)):
+            gather(order[n])
+            if n == 1 and l + 1 < layers:
+                fetched(l + 1, 0)
+            receive(order[n - 1])
+        receive(order[-1])
 
     for c in sends:
         c.wait_send()
@@ -920,7 +934,7 @@
         for k in dp_peers:
             for p in range(4):
                 part(l, p, k).wait_send()
-        for i, k in [(1, 0)] + [(i, k) for k in near_first for i in (0, 1)]:
+        for i, k in [(1, 0)] + [(i, k) for k in turns for i in (0, 1)]:
             remote(
                 h_recv.at[l, 0, 0], h_recv.at[l, i, k], h_rs.at[l, k], at(i, k)
             ).wait_send()
@@ -929,7 +943,7 @@
                 remote(
                     o_send.at[l, k], o_recv.at[l, j, k], o_rs.at[l, k], at(2 * j, 0)
                 ).wait_send()
-            remote(nb.at[l, 0, 0], nb.at[l, 0, 0], n_rs.at[l], at(1, 0)).wait_send()
+            remote(nb.at[l, 0, 0], nb.at[l, 0, 0], n_rs.at[l, k], at(1, 0)).wait_send()
 
 
 def finish(stream, kept_u, kept_m, ssm, stream_out, kept_u_out, kept_m_out, ssm_out, sems):
@@ -1036,7 +1050,7 @@
             pltpu.SemaphoreType.DMA,
             sems(n_dp),
             sems(n_dp),
-            sems(),
+            sems(n_dp),
             pltpu.SemaphoreType.DMA,
             pltpu.SemaphoreType.DMA((2 * max(layers - 1, 1),)),
         ],

time: 40.3 us -> 39.9 us (0.990)
    pallas_call x1, Pallas kernels: 38.6 us -> 38.2 us  [body(): pl.pallas_call(functools.partial(kernel, n_tp, n_dp, d_here * n_dp, group...]
where the time goes in v3:
time: 39.9 us; the launch traced here: 39.7 us
  Pallas kernels  39.1 us (98%)
  between operations  0.65 us (2%)
    pallas_call x1, Pallas kernels, body(): pl.pallas_call(functools.partial(kernel, n_tp, n_dp, d_here * n_dp, group...  38.2 us
    pallas_call x1, Pallas kernels, body(): pl.pallas_call(finish, out_shape=results, in_specs=[vmem] * len(results),...  0.92 us

profile of v3, /device:TPU:0, one launch (start us, length us, event | category | flops | bytes accessed | tf_op | source)
XLA Modules:
  0.0 39.7 jit_solution(17154197665540954396)
XLA Ops:
  0.6 38.2 %mixer.1 = (f32[128,512]{1,0:T(8,128)S(1)}, bf16[2,3,2,256]{3,2,1,0:T(2,128)(2,1)S(1)}, bf16[2,2,3,2,64]{4,3,2,1,0:T(2,128)(2,1)S(1)}, f32[2,2,256,128]{3,2,1,0:T(8,128)S(1)}) custom-call(s32[2]{0:T(128)} %refs_0_.1, bf16[128,512]{1,0:T(8,128)(2,1)} %refs_1_.1, f32[2,512]{1,0:T(2,128)} %refs_2_.1, bf16[2,512,2,256]{3,2,1,0:T(2,128)(2,1)} %refs_3_.1, ...), custom_call_target="tpu_custom_call" | custom-call | tf_op jit(solution)/shard_map/mixer/pallas_call | solution.py:1010
  38.8 0.9 %finish.1 = (f32[128,512]{1,0:T(8,128)}, bf16[2,3,2,256]{3,2,1,0:T(2,128)(2,1)}, bf16[2,2,3,2,64]{4,3,2,1,0:T(2,128)(2,1)}, f32[2,2,256,128]{3,2,1,0:T(8,128)}) custom-call(f32[128,512]{1,0:T(8,128)S(1)} %get-tuple-element.12.stream, bf16[2,3,2,256]{3,2,1,0:T(2,128)(2,1)S(1)} %get-tuple-element.13.kept_u, ...), custom_call_target="tpu_custom_call" | custom-call | tf_op jit(solution)/shard_map/finish/pallas_call | solution.py:1062

commit v4 on v3

--- a/solution.py
+++ b/solution.py
@@ -419,9 +419,9 @@
     (
         stream, kept_u, kept_m, ssm,
         lens, x, scale, w_gate, w_maps, w_step, tap_u, tap_m, bias, rate, skip, gain, cache_u, cache_m, extra_t, state,
-        wout, in_sem, g_sem,
+        wout, g_sem,
         t_send, t_recv, u_send, u_recv, z_send, z_recv, q_send, q_recv, m_send, m_recv, c_send, c_recv, h_recv, o_send, o_recv, nb,
-        padded, padded_m, mrow, mrows, w_rows, w_sorted, w_flat, taps, par, extra,
+        padded, padded_m, mrow, mrows, w_rows, w_sorted, w_flat, w_turned, taps, par, extra,
         out_sem, a_rs, m_rs, c_rs, h_rs, o_rs, n_rs, w_rs, f_rs,
     ) = refs[len(names) :]
     layers, seqs, slots, heads, head_size, n_state, hp_cols, map_cols = shapes
@@ -463,16 +463,21 @@
     for i, j in others:
         pl.semaphore_signal(barrier, inc=1, device_id=at(i, j))
 
+    spare = [
+        *[o_rs.at[layers - 1, k] for k in range(n_dp)], *[h_rs.at[layers - 1, k] for k in range(n_dp)],
+        *[n_rs.at[layers - 1, k] for k in range(n_dp)], *[a_rs.at[layers - 1, p] for p in range(4)],
+        f_rs.at[0], w_rs,
+    ]
     local = {}
     pairs = dict(
         x=x, scale=scale, w_maps=w_maps, w_step=w_step, lens=lens, tap_u=tap_u, tap_m=tap_m, bias=bias, rate=rate,
         skip=skip, gain=gain, cache_u=cache_u, cache_m=cache_m, extra_t=extra_t, state=state,
     )
     for n, name in enumerate(pairs):
-        local[name] = pltpu.make_async_copy(hbm[name], pairs[name], in_sem.at[n])
+        local[name] = pltpu.make_async_copy(hbm[name], pairs[name], spare[n])
     mine = pl.ds(pl.multiple_of(side * half, LANES), half)
     theirs = pl.ds(pl.multiple_of((1 - side) * half, LANES), half)
-    local["wout"] = pltpu.make_async_copy(hbm["wout"].at[:, :, mine], wout.at[:, 0], in_sem.at[len(pairs)])
+    local["wout"] = pltpu.make_async_copy(hbm["wout"].at[:, :, mine], wout.at[:, 0], spare[len(pairs)])
     gate_copies = [
         [
             pltpu.make_async_copy(
@@ -654,7 +659,7 @@
             mask = jnp.concatenate([(slot < lens[s]).astype(F32) for s in range(seqs)], axis=0)
             r, c = grid(rows, rows)
             causal = (over(r, slots) == over(c, slots)) & (c <= r)
-            tri = ones_where(causal)
+            within_sequence = lax.broadcasted_iota(jnp.int32, (rows, LANES), 0) & (slots - 1)
             r, c = grid(LANES, hp_cols)
             ex = ones_where(r == over(c, head_size))
             r, c = grid(hp_cols, LANES)
@@ -699,8 +704,9 @@
         step = jnp.where(lane < heads, step, 0.0)
         logdec = extra_rows[l] * mask - step * jnp.exp(par[l, 1:2, :])
         logdec = jnp.where(lane < heads, logdec, 0.0)
-        parts = dot(tri, jnp.concatenate(thirds(logdec), axis=1))
-        sums = parts[:, :LANES] + parts[:, LANES : 2 * LANES] + parts[:, 2 * LANES :]
+        sums = logdec
+        for n in [2**i for i in range(slots.bit_length()) if 2**i < slots]:
+            sums = sums + jnp.where(within_sequence >= n, pltpu.roll(sums, n, 0), 0.0)
         sums_t = sums.T
         step_t = step.T
         sums_parts, step_parts = thirds(sums), thirds(step)
@@ -713,8 +719,8 @@
             gap = sums[:, h : h + 1] - sums_t[h : h + 1, :]
             segs.append(jnp.exp(jnp.where(causal, gap, -jnp.inf)) * step_t[h : h + 1, :])
 
-        def filter_inputs():
-            proj = (await_part(l, 1) * factor).astype(BF16).astype(F32)
+        def filter_inputs(acc):
+            proj = (acc * factor).astype(BF16).astype(F32)
             for s in range(seqs):
                 padded[l, s, FRONT : FRONT + slots, :] = proj[s * slots : (s + 1) * slots]
             return convolve(padded, taps[l])
@@ -752,8 +758,13 @@
             )
             return b_map, dot(c_map, b_map, 1, 1), carried * grow
 
+        def gate_of(acc):
+            gate = (acc * factor).astype(BF16).astype(F32)
+            return gate * jax.nn.sigmoid(gate)
+
         if l == 0:
-            inp = filter_inputs()
+            inp = filter_inputs(await_part(l, 1))
+            gate = gate_of(await_part(l, 2))
             landed(c_recv.at[1:n_tp], c_rs)
             total = c_recv[0].astype(F32)
             for k in range(1, n_tp):
@@ -763,17 +774,17 @@
                 for s in range(seqs):
                     n = i * per_layer + s * keep
                     padded_m[i, s, FRONT - keep : FRONT, :] = mrows[n : n + keep, :]
-            raw = unpack_maps()
+            maps_in = unpack_maps()
             for i in range(1, layers):
                 for k in [*[2 * j for j in z_peers], 1]:
                     for which in range(2):
                         fetch(i, k, which).start()
                 for which in range(2):
                     w_rows[i, rows_of(tp, which), :] = w_sorted[i, pick_rows(tp, which), :]
-            b_map, cross, carried = filter_maps(raw)
+            b_map, cross, carried = filter_maps(maps_in)
         else:
             b_map, cross, carried = filter_maps(acc[:, LANES:])
-            inp = filter_inputs()
+            inp = filter_inputs(await_part(l, 1))
         inp_b = inp.astype(BF16)
         within = jnp.concatenate(
             [
@@ -783,9 +794,8 @@
             axis=1,
         )
         inner = within + carried + skip_x[l] * inp
-        acc = await_part(l, 2)
-        gate = (acc * factor).astype(BF16).astype(F32)
-        gate = gate * jax.nn.sigmoid(gate)
+        if l > 0:
+            gate = gate_of(await_part(l, 2))
         read = inner * gate
         power = read * read
         p_hi = power.astype(BF16)
@@ -894,7 +904,7 @@
                 return
             squares = jnp.sum(st * st, axis=1, keepdims=True)
             normed = (st * scale[n : n + 1, :]).astype(BF16)
-            tail = dot(normed, w_rows[n], 1, 1)
+            tail = dot(normed, w_turned[l, :, : w_rows.shape[1]])
             tail = jnp.concatenate([with_squares(tail[:, :LANES], squares), tail[:, LANES:]], axis=1)
             t_send[n, block] = tail.astype(BF16)
             if k:
@@ -905,16 +915,20 @@
             z_send[n, block] = dot(normed, w_flat[l, 0]).astype(BF16)
             if k:
                 part(n, 2, k).start()
-            q_send[n, block] = dot(normed, w_sorted[n], 1, 1).astype(BF16)
+            q_send[n, block] = dot(normed, w_turned[l, :, w_rows.shape[1] :]).astype(BF16)
             if k:
                 part(n, 3, k).start()
 
         order = [0, *turns]
         gather(order[0])
-        for n in range(1, len(order)):
+        if l + 1 < layers:
+            fetched(l + 1, 0)
+            w_turned[l, :, : w_rows.shape[1]] = w_rows[l + 1].T
+            w_turned[l, :, w_rows.shape[1] :] = w_sorted[l + 1].T
+        receive(order[0])
+        gather(order[1])
+        for n in range(2, len(order)):
             gather(order[n])
-            if n == 1 and l + 1 < layers:
-                fetched(l + 1, 0)
             receive(order[n - 1])
         receive(order[-1])
 
@@ -948,18 +962,22 @@
 
 def finish(stream, kept_u, kept_m, ssm, stream_out, kept_u_out, kept_m_out, ssm_out, sems):
     pairs = ((ssm, ssm_out), (stream, stream_out), (kept_u, kept_u_out), (kept_m, kept_m_out))
-    copies = [pltpu.make_async_copy(a, b, sems.at[i]) for i, (a, b) in enumerate(pairs)]
-    for c in copies:
-        c.start()
-    for c in copies:
-        c.wait()
-
-
-def fits(n_tp, n_dp, heads, hp_cols, map_cols, n_state, rows, d_here, keep):
+    step = stream.shape[0] // 4
+    for i, j in [(i, j) for i in range(ssm.shape[0]) for j in range(ssm.shape[1])]:
+        pltpu.make_async_copy(ssm.at[i, j], ssm_out.at[i, j], sems.at[0]).start()
+    for i in range(0, stream.shape[0], step):
+        pltpu.make_async_copy(stream.at[i : i + step], stream_out.at[i : i + step], sems.at[1]).start()
+    for i in (2, 3):
+        pltpu.make_async_copy(*pairs[i], sems.at[i]).start()
+    for i, pair in enumerate(pairs):
+        pltpu.make_async_copy(*pair, sems.at[i]).wait()
+
+
+def fits(layers, n_tp, n_dp, heads, hp_cols, map_cols, n_state, rows, d_here, keep):
     groups = map_cols * n_tp // n_state
     powers = all(n & (n - 1) == 0 for n in (n_tp, n_dp, groups, map_cols // groups))
     return (
-        powers and n_tp > 1 and n_dp > 1 and n_tp * n_dp <= 64 and n_tp % groups == 0 and map_cols % groups == 0
+        powers and layers > 1 and n_tp > 2 and n_dp > 2 and n_tp * n_dp <= 64 and n_tp % groups == 0 and map_cols % groups == 0
         and hp_cols % LANES == 0 and 2 * map_cols == LANES and n_state == LANES
         and rows * 2 * (map_cols // groups) == 8 * LANES and d_here % (2 * LANES) == 0
         and keep <= FRONT and heads <= LANES - 2
@@ -980,7 +998,7 @@
     rows = seqs * slots
     d_here = tokens.shape[1]
     keep = convolution_input_cache.shape[2]
-    if not fits(n_tp, n_dp, heads, hp_cols, map_cols, n_state, rows, d_here, keep):
+    if not fits(layers, n_tp, n_dp, heads, hp_cols, map_cols, n_state, rows, d_here, keep):
         return general_body(n_tp, n_dp, *args)
     groups = map_cols * n_tp // n_state
     n_z = n_tp // 2
@@ -1019,7 +1037,6 @@
             pltpu.SMEM(lengths.shape, jnp.int32),
             *held,
             pltpu.VMEM((layers, 2, hp_cols, d_here // 2), BF16),
-            pltpu.SemaphoreType.DMA((len(operands),)),
             sems(),
             *[
                 pltpu.VMEM((layers, n, rows, width), BF16)
@@ -1040,7 +1057,8 @@
             pltpu.VMEM((n_rows, 2 * n_state), F32),
             pltpu.VMEM((layers, LANES + 2 * n_state, d_here), BF16),
             pltpu.VMEM((layers, LANES, d_here), BF16),
-            pltpu.VMEM((max(layers - 1, 1), 2, d_here, hp_cols), BF16),
+            pltpu.VMEM((layers - 1, 2, d_here, hp_cols), BF16),
+            pltpu.VMEM((layers - 1, d_here, 2 * LANES + 2 * n_state), BF16),
             pltpu.VMEM((layers, 8, hp_cols), F32),
             pltpu.VMEM((layers, 8, LANES), F32),
             pltpu.VMEM((layers, LANES, LANES), F32),
@@ -1052,7 +1070,7 @@
             sems(n_dp),
             sems(n_dp),
             pltpu.SemaphoreType.DMA,
-            pltpu.SemaphoreType.DMA((2 * max(layers - 1, 1),)),
+            pltpu.SemaphoreType.DMA((2 * (layers - 1),)),
         ],
         compiler_params=pltpu.CompilerParams(
             collective_id=0, has_side_effects=True, vmem_limit_bytes=32 * 2**20

time: 39.9 us -> 39.9 us (level)
  no operation moved by 1% of the time
where the time goes in v4:
time: 39.9 us; the launch traced here: 39.7 us
  Pallas kernels  39.1 us (98%)
  between operations  0.65 us (2%)
    pallas_call x1, Pallas kernels, body(): pl.pallas_call(functools.partial(kernel, n_tp, n_dp, d_here * n_dp, group...  38.2 us
    pallas_call x1, Pallas kernels, body(): pl.pallas_call(finish, out_shape=results, in_specs=[vmem] * len(results),...  0.9 us

profile of v4, /device:TPU:0, one launch (start us, length us, event | category | flops | bytes accessed | tf_op | source)
XLA Modules:
  0.0 39.7 jit_solution(16031559770220657738)
XLA Ops:
  0.6 38.2 %mixer.1 = (f32[128,512]{1,0:T(8,128)S(1)}, bf16[2,3,2,256]{3,2,1,0:T(2,128)(2,1)S(1)}, bf16[2,2,3,2,64]{4,3,2,1,0:T(2,128)(2,1)S(1)}, f32[2,2,256,128]{3,2,1,0:T(8,128)S(1)}) custom-call(s32[2]{0:T(128)} %refs_0_.1, bf16[128,512]{1,0:T(8,128)(2,1)} %refs_1_.1, f32[2,512]{1,0:T(2,128)} %refs_2_.1, bf16[2,512,2,256]{3,2,1,0:T(2,128)(2,1)} %refs_3_.1, ...), custom_call_target="tpu_custom_call" | custom-call | tf_op jit(solution)/shard_map/mixer/pallas_call | solution.py:1028
  38.8 0.9 %finish.1 = (f32[128,512]{1,0:T(8,128)}, bf16[2,3,2,256]{3,2,1,0:T(2,128)(2,1)}, bf16[2,2,3,2,64]{4,3,2,1,0:T(2,128)(2,1)}, f32[2,2,256,128]{3,2,1,0:T(8,128)}) custom-call(f32[128,512]{1,0:T(8,128)S(1)} %get-tuple-element.12.stream, bf16[2,3,2,256]{3,2,1,0:T(2,128)(2,1)S(1)} %get-tuple-element.13.kept_u, ...), custom_call_target="tpu_custom_call" | custom-call | tf_op jit(solution)/shard_map/finish/pallas_call | solution.py:1080

commit v5 on v4

--- a/solution.py
+++ b/solution.py
@@ -419,7 +419,7 @@
     (
         stream, kept_u, kept_m, ssm,
         lens, x, scale, w_gate, w_maps, w_step, tap_u, tap_m, bias, rate, skip, gain, cache_u, cache_m, extra_t, state,
-        wout, g_sem,
+        wout, g_sem, state_b,
         t_send, t_recv, u_send, u_recv, z_send, z_recv, q_send, q_recv, m_send, m_recv, c_send, c_recv, h_recv, o_send, o_recv, nb,
         padded, padded_m, mrow, mrows, w_rows, w_sorted, w_flat, w_turned, taps, par, extra,
         out_sem, a_rs, m_rs, c_rs, h_rs, o_rs, n_rs, w_rs, f_rs,
@@ -459,9 +459,6 @@
 
     def at(i, j):
         return {"tp": jnp.bitwise_xor(tp, i), "dp": jnp.bitwise_xor(dp, j)}
-
-    for i, j in others:
-        pl.semaphore_signal(barrier, inc=1, device_id=at(i, j))
 
     spare = [
         *[o_rs.at[layers - 1, k] for k in range(n_dp)], *[h_rs.at[layers - 1, k] for k in range(n_dp)],
@@ -492,6 +489,8 @@
         local[name].start()
     for c in gate_copies[0]:
         c.start()
+    for i, j in others:
+        pl.semaphore_signal(barrier, inc=1, device_id=at(i, j))
     for name in local:
         if name not in first:
             local[name].start()
@@ -681,6 +680,7 @@
                     for t in range(keep):
                         n = FRONT - keep + t
                         padded[i, s, n : n + 1, :] = cache_u[i, t].astype(F32)[s : s + 1]
+            state_b[...] = state[...].astype(BF16)
             extra_rows = [extra[i].T[:rows] for i in range(layers)]
             skip_x = [sum(dot(piece, ex) for piece in thirds(par[i]))[2:3] for i in range(layers)]
 
@@ -751,7 +751,7 @@
             b_map, c_map = maps[:, :n_state], maps[:, n_state:]
             carried = jnp.concatenate(
                 [
-                    dot(c_map[s * slots : (s + 1) * slots], state[l, s].astype(BF16), 1, 1)
+                    dot(c_map[s * slots : (s + 1) * slots], state_b[l, s], 1, 1)
                     for s in range(seqs)
                 ],
                 axis=0,
@@ -1038,6 +1038,7 @@
             *held,
             pltpu.VMEM((layers, 2, hp_cols, d_here // 2), BF16),
             sems(),
+            pltpu.VMEM(state.shape, BF16),
             *[
                 pltpu.VMEM((layers, n, rows, width), BF16)
                 for width in (LANES + 2 * n_state, hp_cols, hp_cols, LANES)

time: 39.9 us -> 39.9 us (level)
  no operation moved by 1% of the time
where the time goes in v5:
time: 39.9 us; the launch traced here: 39.7 us
  Pallas kernels  39.1 us (98%)
  between operations  0.65 us (2%)
    pallas_call x1, Pallas kernels, body(): pl.pallas_call(functools.partial(kernel, n_tp, n_dp, d_here * n_dp, group...  38.2 us
    pallas_call x1, Pallas kernels, body(): pl.pallas_call(finish, out_shape=results, in_specs=[vmem] * len(results),...  0.9 us

profile of v5, /device:TPU:0, one launch (start us, length us, event | category | flops | bytes accessed | tf_op | source)
XLA Modules:
  0.0 39.7 jit_solution(15936992508602768202)
XLA Ops:
  0.6 38.2 %mixer.1 = (f32[128,512]{1,0:T(8,128)S(1)}, bf16[2,3,2,256]{3,2,1,0:T(2,128)(2,1)S(1)}, bf16[2,2,3,2,64]{4,3,2,1,0:T(2,128)(2,1)S(1)}, f32[2,2,256,128]{3,2,1,0:T(8,128)S(1)}) custom-call(s32[2]{0:T(128)} %refs_0_.1, bf16[128,512]{1,0:T(8,128)(2,1)} %refs_1_.1, f32[2,512]{1,0:T(2,128)} %refs_2_.1, bf16[2,512,2,256]{3,2,1,0:T(2,128)(2,1)} %refs_3_.1, ...), custom_call_target="tpu_custom_call" | custom-call | tf_op jit(solution)/shard_map/mixer/pallas_call | solution.py:1028
  38.8 0.9 %finish.1 = (f32[128,512]{1,0:T(8,128)}, bf16[2,3,2,256]{3,2,1,0:T(2,128)(2,1)}, bf16[2,2,3,2,64]{4,3,2,1,0:T(2,128)(2,1)}, f32[2,2,256,128]{3,2,1,0:T(8,128)}) custom-call(f32[128,512]{1,0:T(8,128)S(1)} %get-tuple-element.12.stream, bf16[2,3,2,256]{3,2,1,0:T(2,128)(2,1)S(1)} %get-tuple-element.13.kept_u, ...), custom_call_target="tpu_custom_call" | custom-call | tf_op jit(solution)/shard_map/finish/pallas_call | solution.py:1081
